TPU v7x, 256 devices: a whole 4x4x8 slice. The times are simulated.
256 devices in a mesh: ep: 64 (over z, y, core), tp: 4 (over x).
Axes of the slice: x: 4, y: 4, z: 8, core: 2. Of those that a mesh axis runs over, the one named last changes fastest.
Arguments:
- tokens: bfloat16 [1536, 4096], P('ep'), may hold values from -16 to 16
- cotangent: bfloat16 [1536, 4096], P('ep'), may hold values from -1.5 to 1.5
- routes: int32 [1536, 4], P('ep'), may hold values from 0 to 63, all different within a row; in each aligned block of 24 rows (0 to 23, 24 to 47, ...) at most 3 rows name the same one
- route_weights: float32 [1536, 4], P('ep'), may hold values from 0.1 to 1.2
- expert_gate: bfloat16 [64, 4096, 192], P('ep', None, 'tp'), may hold values from -0.09375 to 0.09375
- expert_up: bfloat16 [64, 4096, 192], P('ep', None, 'tp'), may hold values from -0.09375 to 0.09375
- expert_down: bfloat16 [64, 192, 4096], P('ep', 'tp'), may hold values from -0.4375 to 0.4375
- shared_gate: bfloat16 [4096, 192], P(None, 'tp'), may hold values from -0.09375 to 0.09375
- shared_up: bfloat16 [4096, 192], P(None, 'tp'), may hold values from -0.09375 to 0.09375
- shared_down: bfloat16 [192, 4096], P('tp'), may hold values from -0.4375 to 0.4375
Outputs:
- grad_tokens: bfloat16 [1536, 4096], P('ep', 'tp')
- grad_route_weights: float32 [1536, 4], P('ep', 'tp')
- grad_expert_gate: float32 [64, 4096, 192], P('ep', None, 'tp')
- grad_expert_up: float32 [64, 4096, 192], P('ep', None, 'tp')
- grad_expert_down: float32 [64, 192, 4096], P('ep', 'tp')
- grad_shared_gate: float32 [4096, 192], P('ep', 'tp')
- grad_shared_up: float32 [4096, 192], P('ep', 'tp')
- grad_shared_down: float32 [192, 4096], P('tp', 'ep')
Inputs may be any that keep to these rules, and one draw needn't show every extreme that they name: `routes`: each row names 4 different experts of 0 to 63; among the 24 rows of one index of ep (aligned blocks) no expert is named more than 3 times, and in every draw some block names some expert exactly 3 times.
All inputs are finite; a program needn't handle non-finite values.
Results may differ from a plain program's by a relative error of at most 0.015.
Values may be sent and summed in bfloat16 or wider, within the bound.
A program may use at most 64 MiB of HBM per device.

v0:
```python
import jax
import jax.numpy as jnp
from jax import lax
from jax.sharding import PartitionSpec as P


def summed_rows(product, rows, axis):
    whole = product(jnp.int32(0), rows * lax.axis_size(axis))
    return lax.psum_scatter(whole, axis, scatter_dimension=0, tiled=True)


def swish_parts(gate_pre):
    sigma = jax.nn.sigmoid(gate_pre)
    return (gate_pre * sigma, sigma * (1.0 + gate_pre * (1.0 - sigma)))


def contract_rows(left, right):
    return lax.dot_general(
        left, right, (((0,), (0,)), ((), ())), preferred_element_type=jnp.float32
    )


def contract_cols(left, right):
    return lax.dot_general(
        left, right, (((1,), (1,)), ((), ())), preferred_element_type=jnp.float32
    )


def to_expert(array, ep_size, local_experts):
    rest = array.shape[1:]
    split = array.reshape((ep_size, local_experts) + rest)
    moved = jnp.moveaxis(split, 1, 0)
    return moved.reshape((local_experts, ep_size * rest[0]) + rest[1:])


def from_expert(array, ep_size, local_experts):
    rest = array.shape[2:]
    split = array.reshape((local_experts, ep_size, array.shape[1] // ep_size) + rest)
    moved = jnp.moveaxis(split, 0, 1)
    return moved.reshape((ep_size * local_experts, array.shape[1] // ep_size) + rest)


def local(
    tokens,
    cotangent,
    routes,
    route_weights,
    expert_gate,
    expert_up,
    expert_down,
    shared_gate,
    shared_up,
    shared_down,
):
    tok_rows, width = tokens.shape
    top_count = routes.shape[1]
    local_experts = expert_gate.shape[0]
    ep_size = lax.axis_size("ep")
    all_experts = ep_size * local_experts
    capacity = min(tok_rows, tok_rows * top_count // all_experts + 2)
    s_gate = jnp.dot(tokens, shared_gate, preferred_element_type=jnp.float32)
    s_up = jnp.dot(tokens, shared_up, preferred_element_type=jnp.float32)
    s_active, s_slope = swish_parts(s_gate)
    s_hidden = (s_active * s_up).astype(jnp.bfloat16)
    s_back = contract_cols(cotangent, shared_down)
    ds_gate = (s_back * s_up * s_slope).astype(jnp.bfloat16)
    ds_up = (s_back * s_active).astype(jnp.bfloat16)
    shared_dx = contract_cols(ds_gate, shared_gate) + contract_cols(ds_up, shared_up)

    def shared_sums():

        def term(start, count):
            cols_x = lax.dynamic_slice_in_dim(tokens, start, count, 1)
            cols_g = lax.dynamic_slice_in_dim(cotangent, start, count, 1)
            return jnp.concatenate(
                [
                    contract_rows(cols_x, ds_gate),
                    contract_rows(cols_x, ds_up),
                    contract_rows(cols_g, s_hidden),
                ],
                axis=1,
            )

        return summed_rows(term, width // ep_size, "ep")

    flat_routes = routes.reshape(-1)
    assigns = flat_routes.shape[0]
    one_hot = (flat_routes[:, None] == jnp.arange(all_experts, dtype=jnp.int32)[None, :]).astype(
        jnp.int32
    )
    earlier = jnp.cumsum(one_hot, axis=0) - one_hot
    position = jnp.sum(earlier * one_hot, axis=1)
    target = flat_routes * capacity + position
    slot_source = (
        jnp.zeros((all_experts * capacity,), jnp.int32)
        .at[target]
        .set(jnp.arange(assigns, dtype=jnp.int32) + 1)
    )
    filled = slot_source > 0
    slot_token = jnp.where(filled, (slot_source - 1) // top_count, tok_rows)
    slot_assign = jnp.where(filled, slot_source - 1, assigns)
    padded_x = jnp.concatenate([tokens, jnp.zeros((1, width), tokens.dtype)], axis=0)
    padded_g = jnp.concatenate([cotangent, jnp.zeros((1, width), cotangent.dtype)], axis=0)
    padded_w = jnp.concatenate([route_weights.reshape(-1), jnp.zeros((1,), jnp.float32)], axis=0)
    send_x = padded_x[slot_token].reshape(all_experts, capacity, width)
    send_g = padded_g[slot_token].reshape(all_experts, capacity, width)
    send_w = padded_w[slot_assign].reshape(all_experts, capacity)
    recv_x, recv_g = (
        lax.all_to_all(send_x, "ep", split_axis=0, concat_axis=0, tiled=True),
        lax.all_to_all(send_g, "ep", split_axis=0, concat_axis=0, tiled=True),
    )
    recv_w = lax.all_to_all(send_w, "ep", split_axis=0, concat_axis=0, tiled=True)
    rows_x = to_expert(recv_x, ep_size, local_experts)
    rows_g = to_expert(recv_g, ep_size, local_experts)
    rows_w = to_expert(recv_w, ep_size, local_experts)
    e_gate = jnp.einsum("erd,edf->erf", rows_x, expert_gate, preferred_element_type=jnp.float32)
    e_up = jnp.einsum("erd,edf->erf", rows_x, expert_up, preferred_element_type=jnp.float32)
    e_active, e_slope = swish_parts(e_gate)
    e_hidden = (e_active * e_up).astype(jnp.bfloat16)
    e_back = jnp.einsum("erd,efd->erf", rows_g, expert_down, preferred_element_type=jnp.float32)
    gate_part = jnp.sum(e_hidden.astype(jnp.float32) * e_back, axis=-1)
    d_hidden = rows_w[..., None] * e_back
    de_gate = (d_hidden * e_up * e_slope).astype(jnp.bfloat16)
    de_up = (d_hidden * e_active).astype(jnp.bfloat16)
    scaled = (rows_w[..., None] * e_hidden.astype(jnp.float32)).astype(jnp.bfloat16)
    grad_down = jnp.einsum("erf,erd->efd", scaled, rows_g, preferred_element_type=jnp.float32)
    grad_gate = jnp.einsum("erd,erf->edf", rows_x, de_gate, preferred_element_type=jnp.float32)
    grad_up = jnp.einsum("erd,erf->edf", rows_x, de_up, preferred_element_type=jnp.float32)
    dx_part = jnp.einsum("erf,edf->erd", de_gate, expert_gate, preferred_element_type=jnp.float32)
    dx_part = dx_part + jnp.einsum(
        "erf,edf->erd", de_up, expert_up, preferred_element_type=jnp.float32
    )
    dx_sent = from_expert(dx_part, ep_size, local_experts)
    gate_sent = from_expert(gate_part, ep_size, local_experts)[..., None]
    back_dx, back_gate = (
        lax.all_to_all(
            dx_sent.astype(jnp.bfloat16), "ep", split_axis=0, concat_axis=0, tiled=True
        ).astype(dx_sent.dtype),
        lax.all_to_all(
            gate_sent.astype(jnp.bfloat16), "ep", split_axis=0, concat_axis=0, tiled=True
        ).astype(gate_sent.dtype),
    )
    routed = back_dx.reshape(all_experts * capacity, width)[target]
    routed = jnp.sum(routed.reshape(tok_rows, top_count, width), axis=1)
    gate_full = back_gate.reshape(all_experts * capacity)[target].reshape(tok_rows, top_count)
    token_sum, grad_route = (
        lax.psum_scatter(
            (routed + shared_dx).astype(jnp.bfloat16), "tp", scatter_dimension=1, tiled=True
        ).astype(jnp.float32),
        lax.psum_scatter(
            gate_full.astype(jnp.bfloat16), "tp", scatter_dimension=1, tiled=True
        ).astype(jnp.float32),
    )
    grad_tokens = token_sum.astype(jnp.bfloat16)
    shared_total = shared_sums()
    hidden_local = shared_gate.shape[1]
    grad_shared_gate = shared_total[:, :hidden_local]
    grad_shared_up = shared_total[:, hidden_local : 2 * hidden_local]
    grad_shared_down = shared_total[:, 2 * hidden_local :].T
    return (
        grad_tokens,
        grad_route,
        grad_gate,
        grad_up,
        grad_down,
        grad_shared_gate,
        grad_shared_up,
        grad_shared_down,
    )


def solution(mesh):
    placed = (
        P("ep", None),
        P("ep", None),
        P("ep", None),
        P("ep", None),
        P("ep", None, "tp"),
        P("ep", None, "tp"),
        P("ep", "tp", None),
        P(None, "tp"),
        P(None, "tp"),
        P("tp", None),
    )
    return jax.shard_map(
        local,
        mesh=mesh,
        in_specs=placed,
        out_specs=(
            P("ep", "tp"),
            P("ep", "tp"),
            P("ep", None, "tp"),
            P("ep", None, "tp"),
            P("ep", "tp", None),
            P("ep", "tp"),
            P("ep", "tp"),
            P("tp", "ep"),
        ),
        check_vma=False,
    )
```

profile of v0, /device:TPU:1, one launch (start us, length us, event | category | flops | bytes accessed | tf_op | source)
XLA Modules:
  0.0 295.5 jit_solution(8192158157360182437)
XLA Ops:
  7.2 0.8 copy.28
  9.4 0.9 scatter_custom_fusion
  10.3 0.8 copy.26
  11.3 1.5 gather_fusion
  12.9 0.8 all_to_all.18
  13.6 13.2 %all-to-all-start = ((f32[64,1,3]{2,1,0:T(1,128)}), f32[64,1,3]{2,1,0:T(1,128)S(1)}, u32[]{:S(2)}, u32[]{:S(2)}) async-start(f32[64,1,3]{2,1,0:T(1,128)} %bitcast.2), calls=%async_computation | async-start | bytes 65536 | tf_op jit(solution)/shard_map/all_to_all | solution.py:112
  26.8 1.5 gather_fusion.2
  28.3 2.3 reshape.168
  30.6 6.0 %all-to-all-done = f32[64,1,3]{2,1,0:T(1,128)S(1)} async-done(((f32[64,1,3]{2,1,0:T(1,128)}), f32[64,1,3]{2,1,0:T(1,128)S(1)}, u32[]{:S(2)}, u32[]{:S(2)}) %all-to-all-start) | async-done | bytes 800 | tf_op jit(solution)/shard_map/all_to_all | solution.py:112
  37.2 4.8 %all-to-all-start.2 = ((bf16[64,3,4096]{2,1,0:T(4,128)(2,1)}), bf16[64,3,4096]{2,1,0:T(4,128)(2,1)S(1)}, u32[]{:S(2)}, u32[]{:S(2)}) async-start(bf16[64,3,4096]{2,1,0:T(4,128)(2,1)} %reshape.168), calls=%async_computation.2 | async-start | bytes 4194304 | tf_op jit(solution)/shard_map/all_to_all | solution.py:109
  42.1 2.7 gather_fusion.1
  44.8 4.1 %reshape.165 = bf16[64,3,4096]{2,1,0:T(4,128)(2,1)} reshape(bf16[192,4096]{1,0:T(8,128)(2,1)} %gather_fusion.1) | data formatting | bytes 3145728 | tf_op jit(solution)/shard_map/reshape | solution.py:106
  48.8 45.1 %all-to-all-done.2 = bf16[64,3,4096]{2,1,0:T(4,128)(2,1)S(1)} async-done(((bf16[64,3,4096]{2,1,0:T(4,128)(2,1)}), bf16[64,3,4096]{2,1,0:T(4,128)(2,1)S(1)}, u32[]{:S(2)}, u32[]{:S(2)}) %all-to-all-start.2) | async-done | bytes 1572896 | tf_op jit(solution)/shard_map/all_to_all | solution.py:109
  93.9 1.4 copy-done.1
  95.2 5.7 %all-to-all-start.1 = ((bf16[64,3,4096]{2,1,0:T(4,128)(2,1)}), bf16[64,3,4096]{2,1,0:T(4,128)(2,1)}, u32[]{:S(2)}, u32[]{:S(2)}) async-start(bf16[64,3,4096]{2,1,0:T(4,128)(2,1)} %reshape.165), calls=%async_computation.1 | async-start | bytes 4194304 | tf_op jit(solution)/shard_map/all_to_all | solution.py:110
  101.0 1.2 fusion.25
  102.4 1.2 multiply_convert_fusion.4
  104.8 3.3 %copy.33 = f32[4096,144]{1,0:T(8,128)} copy(f32[4096,144]{0,1:T(8,128)S(1)} %pad_maximum_fusion) | data formatting | bytes 4718592
  110.2 3.1 %reshape.169 = bf16[192,4096]{1,0:T(8,128)(2,1)S(1)} reshape(bf16[64,3,4096]{2,1,0:T(4,128)(2,1)} %copy-done.1) | data formatting | bytes 3145728 | tf_op jit(solution)/shard_map/reshape.4
  113.4 1.2 fusion.5
  114.6 1.2 fusion.8
  115.9 35.2 %all-to-all-done.1 = bf16[64,3,4096]{2,1,0:T(4,128)(2,1)} async-done(((bf16[64,3,4096]{2,1,0:T(4,128)(2,1)}), bf16[64,3,4096]{2,1,0:T(4,128)(2,1)}, u32[]{:S(2)}, u32[]{:S(2)}) %all-to-all-start.1) | async-done | bytes 1572896 | tf_op jit(solution)/shard_map/all_to_all | solution.py:110
  151.1 3.1 %reshape.166 = bf16[192,4096]{1,0:T(8,128)(2,1)S(1)} reshape(bf16[64,3,4096]{2,1,0:T(4,128)(2,1)} %all-to-all-done.1) | data formatting | bytes 3145728 | tf_op jit(solution)/shard_map/reshape.1
  154.2 2.7 fusion.12
  157.9 1.8 fusion
  159.7 4.1 %convert_element_type.73 = bf16[64,3,4096]{2,1,0:T(4,128)(2,1)} reshape(bf16[192,4096]{1,0:T(8,128)(2,1)} %fusion) | data formatting | bytes 3145728 | tf_op jit(solution)/shard_map/convert_element_type | solution.py:137
  163.8 7.3 %all-to-all-start.3 = ((bf16[64,3,4096]{2,1,0:T(4,128)(2,1)}), bf16[64,3,4096]{2,1,0:T(4,128)(2,1)}, u32[]{:S(2)}, u32[]{:S(2)}) async-start(bf16[64,3,4096]{2,1,0:T(4,128)(2,1)} %convert_element_type.73), calls=%async_computation.3 | async-start | bytes 4194304 | tf_op jit(solution)/shard_map/all_to_all | solution.py:136
  171.1 1.3 dynamic-slice
  172.4 1.3 pad_clamp_fusion
  173.7 2.0 fusion.27
  175.7 1.4 convert_element_type.86
  177.1 2.0 convolution_bitcast_fusion
  179.1 1.3 convolution_bitcast_fusion.1
  180.4 1.3 convolution_bitcast_fusion.5
  181.7 50.0 %all-to-all-done.3 = bf16[64,3,4096]{2,1,0:T(4,128)(2,1)} async-done(((bf16[64,3,4096]{2,1,0:T(4,128)(2,1)}), bf16[64,3,4096]{2,1,0:T(4,128)(2,1)}, u32[]{:S(2)}, u32[]{:S(2)}) %all-to-all-start.3) | async-done | bytes 1572896 | tf_op jit(solution)/shard_map/all_to_all | solution.py:136
  231.7 6.1 %all-to-all-start.4 = ((bf16[64,3,1]{1,2,0:T(2,128)(2,1)}), bf16[64,3,1]{1,2,0:T(2,128)(2,1)}, u32[]{:S(2)}, u32[]{:S(2)}) async-start(bf16[64,3,1]{1,2,0:T(2,128)(2,1)} %convert_element_type.86), calls=%async_computation.5 | async-start | bytes 65536 | tf_op jit(solution)/shard_map/all_to_all | solution.py:139
  237.9 3.0 %reshape.178 = f32[192,4096]{1,0:T(8,128)S(1)} reshape(bf16[64,3,4096]{2,1,0:T(4,128)(2,1)} %all-to-all-done.3) | data formatting | bytes 4718592 | tf_op jit(solution)/shard_map/reshape | solution.py:143
  240.9 2.3 gather_fusion.3
  243.2 1.7 reshape.174
  245.0 0.9 reduce_sum.31
  246.1 0.9 fusion.2
  247.0 1.0 all-to-all-done.4
  248.0 0.9 convert_reduce_fusion
  249.0 1.4 gather_fusion.4
  250.5 9.2 %all-reduce.2 = bf16[24,4]{1,0:T(8,128)(2,1)S(1)} all-reduce(bf16[24,4]{1,0:T(8,128)(2,1)S(1)} %convert_element_type.82), channel_id=3, replica_groups=mesh['ep'=64,'tp'=4] {'tp'}, use_global_device_ids=true, to_apply=%region_6.7.clone | all-reduce | flops 96 | bytes 384
  261.0 1.1 reduce-scatter.8.cloned.1.call-done
  262.1 1.0 fusion.24
  265.2 23.5 %reduce-scatter.6.cloned.1.call-done = bf16[24,1024]{1,0:T(8,128)(2,1)} async-done(((bf16[24,4096]{1,0:T(8,128)(2,1)}), bf16[24,1024]{1,0:T(8,128)(2,1)}) %reduce-scatter.6.cloned.1.call-update) | async-done | bytes 49168 | tf_op jit(solution)/shard_map/reduce_scatter | solution.py:147
  (68 shorter events, 10.6 us)
Async XLA Ops:
  7.2 106.2 %copy-start = (bf16[1,4096,48]{1,2,0:T(8,128)(2,1)S(1)}, bf16[1,4096,48]{1,2,0:T(8,128)(2,1)}, u32[]{:S(2)}) copy-start(bf16[1,4096,48]{1,2,0:T(8,128)(2,1)} %param.14) | copy-start | bytes 1179652
  7.2 19.6 %copy-start.2 = (bf16[24,4096]{1,0:T(8,128)(2,1)S(1)}, bf16[24,4096]{1,0:T(8,128)(2,1)}, u32[]{:S(2)}) copy-start(bf16[24,4096]{1,0:T(8,128)(2,1)} %param.10) | copy-start | bytes 589828
  9.4 0.9 copy-start.16
  13.6 23.0 %all-to-all-start = ((f32[64,1,3]{2,1,0:T(1,128)}), f32[64,1,3]{2,1,0:T(1,128)S(1)}, u32[]{:S(2)}, u32[]{:S(2)}) async-start(f32[64,1,3]{2,1,0:T(1,128)} %bitcast.2), calls=%async_computation | async-start | bytes 65536 | tf_op jit(solution)/shard_map/all_to_all | solution.py:112
  30.6 11.4 %copy-start.3 = (bf16[24,4096]{1,0:T(8,128)(2,1)S(1)}, bf16[24,4096]{1,0:T(8,128)(2,1)}, u32[]{:S(2)}) copy-start(bf16[24,4096]{1,0:T(8,128)(2,1)} %param.11) | copy-start | bytes 589828
  36.6 0.6 copy-start.12
  37.2 56.6 %all-to-all-start.2 = ((bf16[64,3,4096]{2,1,0:T(4,128)(2,1)}), bf16[64,3,4096]{2,1,0:T(4,128)(2,1)S(1)}, u32[]{:S(2)}, u32[]{:S(2)}) async-start(bf16[64,3,4096]{2,1,0:T(4,128)(2,1)} %reshape.168), calls=%async_computation.2 | async-start | bytes 4194304 | tf_op jit(solution)/shard_map/all_to_all | solution.py:109
  48.8 53.3 %copy-start.4 = (bf16[4096,48]{0,1:T(8,128)(2,1)S(1)}, bf16[4096,48]{0,1:T(8,128)(2,1)}, u32[]{:S(2)}) copy-start(bf16[4096,48]{0,1:T(8,128)(2,1)} %param.17) | copy-start | bytes 1179652
  93.9 1.4 copy-start.1
  95.2 55.8 %all-to-all-start.1 = ((bf16[64,3,4096]{2,1,0:T(4,128)(2,1)}), bf16[64,3,4096]{2,1,0:T(4,128)(2,1)}, u32[]{:S(2)}, u32[]{:S(2)}) async-start(bf16[64,3,4096]{2,1,0:T(4,128)(2,1)} %reshape.165), calls=%async_computation.1 | async-start | bytes 4194304 | tf_op jit(solution)/shard_map/all_to_all | solution.py:110
  100.9 161.2 %reduce-scatter.8.cloned.1.call-start = ((), (), s32[]{:S(2)}) async-start(), calls=%async_computation.8 | async-start | bytes 4259840
  108.0 0.8 copy-start.13
  113.4 1.3 copy-start.7
  156.9 0.6 copy-start.9
  156.9 0.6 copy-start.11
  156.9 1.0 copy-start.8
  163.8 67.9 %all-to-all-start.3 = ((bf16[64,3,4096]{2,1,0:T(4,128)(2,1)}), bf16[64,3,4096]{2,1,0:T(4,128)(2,1)}, u32[]{:S(2)}, u32[]{:S(2)}) async-start(bf16[64,3,4096]{2,1,0:T(4,128)(2,1)} %convert_element_type.73), calls=%async_computation.3 | async-start | bytes 4194304 | tf_op jit(solution)/shard_map/all_to_all | solution.py:136
  177.1 2.0 copy-start.10
  179.1 1.3 copy-start.14
  179.1 1.3 copy-start.15
  231.7 16.3 %all-to-all-start.4 = ((bf16[64,3,1]{1,2,0:T(2,128)(2,1)}), bf16[64,3,1]{1,2,0:T(2,128)(2,1)}, u32[]{:S(2)}, u32[]{:S(2)}) async-start(bf16[64,3,1]{1,2,0:T(2,128)(2,1)} %convert_element_type.86), calls=%async_computation.5 | async-start | bytes 65536 | tf_op jit(solution)/shard_map/all_to_all | solution.py:139
  237.8 50.9 %reduce-scatter.6.cloned.1.call-start = ((), (), s32[]{:S(2)}) async-start(), calls=%async_computation.7 | async-start | bytes 245760 | tf_op jit(solution)/shard_map/reduce_scatter | solution.py:147
  245.0 1.0 copy-start.5
  245.0 1.1 copy-start.6
Sparse Core Ops, SparseCore 0:
  108.2 153.8 reduce-scatter.7
  265.2 23.4 reduce-scatter.5
where the time goes:
time: 298 us; the launch traced here: 296 us
  waiting for transfers between devices  162 us (54%)
  local copies, waits for them, and re-layouts  48.6 us (16%)
  starting transfers between devices  37.1 us (12%)
  matrix products  18.5 us (6%)
  between operations  14.4 us (5%)
  blocking collectives  9.19 us (3%)
  other arithmetic  5.87 us (2%)
    all_to_all x1, waiting for transfers between devices, local(): lax.all_to_all(dx_sent.astype(jnp.bfloat16), 'ep', split_axis=0, concat_a...  50 us
    all_to_all x1, waiting for transfers between devices, local(): lax.all_to_all(send_x, 'ep', split_axis=0, concat_axis=0, tiled=True)  45.1 us
    all_to_all x1, waiting for transfers between devices, local(): lax.all_to_all(send_g, 'ep', split_axis=0, concat_axis=0, tiled=True)  35.2 us
    reduce_scatter x1, waiting for transfers between devices, local(): lax.psum_scatter((routed + shared_dx).astype(jnp.bfloat16), 'tp', scatter...  23.5 us
    all_to_all x1, starting transfers between devices, local(): lax.all_to_all(send_w, 'ep', split_axis=0, concat_axis=0, tiled=True)  13.2 us
    unnamed x42, local copies, waits for them, and re-layouts  11.6 us
    unnamed x1, blocking collectives  9.19 us
    all_to_all x1, starting transfers between devices, local(): lax.all_to_all(dx_sent.astype(jnp.bfloat16), 'ep', split_axis=0, concat_a...  7.32 us
  transfers between devices with their start and end apart: 7, of which 7 were waited for; matrix products, arithmetic and copies ran while one was open for 22% of the time, Pallas kernels for 0%

commit v1 on v0

v1 whole, which is shorter than its diff:
```python
import functools

import jax
import jax.numpy as jnp
from jax import lax
from jax.experimental import pallas as pl
from jax.experimental.pallas import tpu as pltpu
from jax.sharding import PartitionSpec as P

MESH = pl.DeviceIdType.MESH
F32 = jnp.float32
BF16 = jnp.bfloat16
EP_AXES = (8, 4, 2)
CAP = 3


def dot_nn(a, b):
    return lax.dot_general(a, b, (((1,), (0,)), ((), ())), preferred_element_type=F32)


def dot_nt(a, b):
    return lax.dot_general(a, b, (((1,), (1,)), ((), ())), preferred_element_type=F32)


def dot_tn(a, b):
    return lax.dot_general(a, b, (((0,), (0,)), ((), ())), preferred_element_type=F32)


def wait_bytes(ref, sem):
    pltpu.make_async_copy(ref, ref, sem).wait()


def swish_parts(v):
    sigma = jax.nn.sigmoid(v)
    return v * sigma, sigma * (1.0 + v * (1.0 - sigma))


def swap_matrix(outer, inner):
    size = outer * inner
    row = lax.broadcasted_iota(jnp.int32, (size, size), 0)
    col = lax.broadcasted_iota(jnp.int32, (size, size), 1)
    return ((row % inner) * outer + row // inner == col).astype(BF16)


def kernel(
    sizes,
    assign_of,
    slot_of,
    weight_of,
    x_ref,
    g_ref,
    wg_ref,
    wu_ref,
    wd_ref,
    sg_ref,
    su_ref,
    sd_ref,
    dx_out,
    gr_out,
    gw_out,
    gs_out,
    tiles,
    send_x,
    recv_x,
    wq,
    rows,
    part,
    rs_send,
    rs_recv,
    dall,
    back_send,
    back_recv,
    gp_send,
    gp_recv,
    dw_send,
    sdx_send,
    sdx_recv,
    sh1,
    sh1_recv,
    sh2,
    sh2_recv,
    sh3,
    sh3_recv,
    sh4,
    sh4_recv,
    comb,
    grow,
    sem,
):
    ep, tp, nz, ny, cap, tok, top, dq, ff, cb = sizes
    nb = dq // 128
    slots = ep * cap
    own_rows = slots // tp
    fo = ff // tp
    chunk = cap * 2 * nb
    me = lax.axis_index("ep")
    q = lax.axis_index("tp")
    core = lax.rem(me, 2)
    yy = lax.rem(me // 2, ny)
    zz = me // (2 * ny)
    sib = me + 1 - 2 * core

    def ep_peer(i):
        return lax.rem(me + i, ep)

    def tp_peer(i):
        return lax.rem(q + i, tp)

    def send(src, dst, kind, device):
        pltpu.make_async_remote_copy(
            src_ref=src,
            dst_ref=dst,
            send_sem=sem.at[2 * kind],
            recv_sem=sem.at[2 * kind + 1],
            device_id=device,
            device_id_type=MESH,
        ).start()

    def waits(ref, kind, side):
        wait_bytes(ref, sem.at[2 * kind + side])

    barrier = pltpu.get_barrier_semaphore()

    @pl.loop(1, ep)
    def _(i):
        pl.semaphore_signal(barrier, inc=1, device_id={"ep": ep_peer(i)}, device_id_type=MESH)

    for i in range(1, tp):
        pl.semaphore_signal(barrier, inc=1, device_id={"tp": tp_peer(i)}, device_id_type=MESH)

    col0 = q * dq
    swap_in = swap_matrix(2 * nb, 16)
    swap_out = swap_matrix(16, 2 * nb)
    for part_no in range(2):
        lo = part_no * 16
        hi = min(tok, lo + 16)
        pieces = []
        for ref in (x_ref, g_ref):
            for b in range(nb):
                cols = pl.ds(pl.multiple_of(col0 + b * 128, 128), 128)
                piece = ref[lo:hi, cols].astype(F32)
                if hi - lo < 16:
                    piece = jnp.concatenate([piece, jnp.zeros((16 - hi + lo, 128), F32)], axis=0)
                pieces.append(piece)
        stacked = jnp.concatenate(pieces, axis=0).astype(BF16)
        moved = dot_nn(swap_out, stacked)
        tiles[lo : lo + 16] = moved.reshape(16, 2 * nb, 128)

    lower = lax.broadcasted_iota(jnp.int32, (2 * nb, 128), 0) < nb

    @pl.loop(0, slots, unroll=4)
    def _(s):
        a = assign_of[s]
        tile = tiles[a // top]
        scale = jnp.where(lower, jnp.float32(1.0), weight_of[a])
        send_x[pl.ds(pl.multiple_of(s * 2 * nb, 2 * nb), 2 * nb), :] = (tile * scale).astype(BF16)

    pl.semaphore_wait(barrier, ep - 1 + tp - 1)

    def chunk_of(i, size):
        return pl.ds(pl.multiple_of(i * size, size), size)

    for t, ref in enumerate((wg_ref, wu_ref, wd_ref)):
        for i in range(1, tp):
            dst_rows = pl.ds(pl.multiple_of(t * ff + q * fo, 16), fo)
            src_cols = pl.ds(pl.multiple_of(tp_peer(i) * dq, 128), dq)
            send(ref.at[:, src_cols], wq.at[dst_rows, :], 0, {"tp": tp_peer(i)})

    @pl.loop(1, ep)
    def _(i):
        p = ep_peer(i)
        send(send_x.at[chunk_of(p, chunk), :], recv_x.at[chunk_of(me, chunk), :], 1, {"ep": p})

    recv_x[chunk_of(me, chunk), :] = send_x[chunk_of(me, chunk), :]
    own_cols = pl.ds(pl.multiple_of(q * dq, 128), dq)
    for t, ref in enumerate((wg_ref, wu_ref, wd_ref)):
        wq[pl.ds(pl.multiple_of(t * ff + q * fo, 16), fo), :] = ref[:, own_cols]

    x = x_ref[...]
    g = g_ref[...]
    s_gate = dot_nt(x, sg_ref[...])
    s_up = dot_nt(x, su_ref[...])
    s_back = dot_nt(g, sd_ref[...])
    s_active, s_slope = swish_parts(s_gate)
    s_hidden = (s_active * s_up).astype(BF16)
    ds_gate = (s_back * s_up * s_slope).astype(BF16)
    ds_up = (s_back * s_active).astype(BF16)
    for j in range(tp):
        cols = slice(j * dq, (j + 1) * dq)
        piece = dot_nn(ds_gate, sg_ref[:, cols]) + dot_nn(ds_up, su_ref[:, cols])
        sdx_send[j] = piece.astype(BF16)
    for i in range(1, tp):
        send(sdx_send.at[tp_peer(i)], sdx_recv.at[q], 2, {"tp": tp_peer(i)})
    half = 3 * fo // 2
    for z in range(nz):
        cols = slice(z * ny * cb, (z + 1) * ny * cb)
        xz = x_ref[:, cols]
        whole = jnp.concatenate(
            [dot_tn(ds_gate, xz), dot_tn(ds_up, xz), dot_tn(s_hidden, g_ref[:, cols])], axis=0
        )
        for y in range(ny):
            for h in range(2):
                sh1[h, y, z] = whole[h * half : (h + 1) * half, y * cb : (y + 1) * cb].astype(BF16)
    send(sh1.at[1 - core], sh1_recv, 3, {"ep": sib})
    waits(sh1_recv, 3, 1)
    for y in range(ny):
        for z in range(nz):
            both = sh1[core, y, z].astype(F32) + sh1_recv[y, z].astype(F32)
            sh2[y, z] = both.astype(BF16)
    for i in range(1, ny):
        y = lax.rem(yy + i, ny)
        send(sh2.at[y], sh2_recv.at[yy], 4, {"ep": (zz * ny + y) * 2 + core})
    if ny > 1:
        waits(sh2_recv.at[pl.ds(0, ny - 1)], 4, 1)
    for z in range(nz):
        total = sh2[yy, z].astype(F32)
        for i in range(1, ny):
            total = total + sh2_recv[lax.rem(yy + i, ny), z].astype(F32)
        sh3[z] = total.astype(BF16)
    for i in range(1, nz):
        z = lax.rem(zz + i, nz)
        send(sh3.at[z], sh3_recv.at[zz], 5, {"ep": (z * ny + yy) * 2 + core})

    waits(wq.at[pl.ds(0, 3 * (tp - 1) * fo), :], 0, 1)
    waits(recv_x.at[pl.ds(0, (ep - 1) * chunk), :], 1, 1)

    @pl.loop(0, slots // 16)
    def _(i):
        block = recv_x[pl.ds(pl.multiple_of(i * 32 * nb, 32 * nb), 32 * nb), :]
        moved = dot_nn(swap_in, block).astype(BF16)
        for b in range(2 * nb):
            rows[pl.ds(pl.multiple_of(i * 16, 16), 16), b * 128 : (b + 1) * 128] = moved[b * 16 : (b + 1) * 16]

    xr = rows[:, 0:dq]
    gr = rows[:, dq : 2 * dq]
    up_part = dot_nt(xr, wq[0 : 2 * ff, :])
    back_part = dot_nt(gr, wq[2 * ff : 3 * ff, :])
    part[:, 0 : 2 * ff] = up_part
    part[:, 2 * ff : 3 * ff] = back_part
    rs_send[:, 0 : 2 * ff] = up_part.astype(BF16)
    rs_send[:, 2 * ff : 3 * ff] = back_part.astype(BF16)
    for i in range(1, tp):
        send(rs_send.at[chunk_of(tp_peer(i), own_rows), :], rs_recv.at[chunk_of(q, own_rows), :], 6, {"tp": tp_peer(i)})
    waits(rs_recv.at[pl.ds(0, (tp - 1) * own_rows), :], 6, 1)
    total = part[chunk_of(q, own_rows), :]
    for i in range(1, tp):
        total = total + rs_recv[chunk_of(tp_peer(i), own_rows), :].astype(F32)
    gate = total[:, 0:ff]
    up = total[:, ff : 2 * ff]
    back = total[:, 2 * ff : 3 * ff]
    active, slope = swish_parts(gate)
    hidden = (active * up).astype(BF16)
    gp = jnp.sum(hidden.astype(F32) * back, axis=1, keepdims=True)
    d_gate = back * up * slope
    d_up = back * active
    extra = dall.shape[1] - 3 * ff
    dall[chunk_of(q, own_rows), :] = jnp.concatenate(
        [d_gate, d_up, hidden.astype(F32), jnp.broadcast_to(gp, (own_rows, extra))], axis=1
    ).astype(BF16)
    for i in range(1, tp):
        mine = dall.at[chunk_of(q, own_rows), :]
        send(mine, mine, 7, {"tp": tp_peer(i)})
    waits(dall.at[pl.ds(0, (tp - 1) * own_rows), :], 7, 1)

    dgu = dall[:, 0 : 2 * ff]
    dh = dall[:, 2 * ff : 3 * ff]
    swap_back = swap_matrix(16, nb)
    dxr = dot_nn(dgu, wq[0 : 2 * ff, :])
    for i in range(slots // 16):
        stacked = jnp.concatenate(
            [dxr[i * 16 : (i + 1) * 16, b * 128 : (b + 1) * 128] for b in range(nb)], axis=0
        ).astype(BF16)
        moved = dot_nn(swap_back, stacked)
        back_send[i * 16 : (i + 1) * 16] = moved.reshape(16, nb, 128).astype(BF16)
    src_row = lax.broadcasted_iota(jnp.int32, (ep, slots), 0)
    src_col = lax.broadcasted_iota(jnp.int32, (ep, slots), 1)
    collect = (src_col // cap == src_row).astype(F32)
    lane = lax.broadcasted_iota(jnp.int32, (slots, 128), 1)
    slot_row = lax.broadcasted_iota(jnp.int32, (slots, 128), 0)
    gp_all = dall[:, 3 * ff : 3 * ff + 1].astype(F32)
    spread = jnp.where(lane == slot_row % cap, gp_all, 0.0)
    gp_rows = dot_nn(collect, spread)
    gp_send[...] = gp_rows.reshape(ep, 1, 128)

    @pl.loop(1, ep)
    def _(i):
        p = ep_peer(i)
        send(back_send.at[pl.ds(p * cap, cap)], back_recv.at[pl.ds(me * cap, cap)], 8, {"ep": p})
        send(gp_send.at[p], gp_recv.at[me], 9, {"ep": p})

    back_recv[pl.ds(me * cap, cap)] = back_send[pl.ds(me * cap, cap)]
    gp_recv[me] = gp_send[me]

    dw_send[0 : 2 * ff, :] = dot_tn(dgu, rows[:, 0:dq]).astype(BF16)
    dw_send[2 * ff : 3 * ff, :] = dot_tn(dh, rows[:, dq : 2 * dq]).astype(BF16)
    for t in range(3):
        for i in range(1, tp):
            src_rows = pl.ds(pl.multiple_of(t * ff + tp_peer(i) * fo, 16), fo)
            send(dw_send.at[src_rows, :], gw_out.at[t, :, own_cols], 10, {"tp": tp_peer(i)})
        mine = pl.ds(pl.multiple_of(t * ff + q * fo, 16), fo)
        gw_out[t, :, own_cols] = dw_send[mine, :]

    if nz > 1:
        waits(sh3_recv.at[pl.ds(0, nz - 1)], 5, 1)
    total = sh3[zz].astype(F32)
    for i in range(1, nz):
        total = total + sh3_recv[lax.rem(zz + i, nz)].astype(F32)
    sh4[...] = total
    send(sh4, sh4_recv, 11, {"ep": sib})
    waits(sh4_recv, 11, 1)
    first = core == 0
    full = jnp.concatenate(
        [
            jnp.where(first, sh4[...], sh4_recv[...]),
            jnp.where(first, sh4_recv[...], sh4[...]),
        ],
        axis=0,
    )
    gs_out[...] = jnp.where(first, full[:, 0 : cb // 2], full[:, cb // 2 : cb])

    waits(sdx_recv.at[pl.ds(0, tp - 1)], 2, 1)
    waits(back_recv.at[pl.ds(0, (ep - 1) * cap)], 8, 1)
    waits(gp_recv.at[pl.ds(0, ep - 1)], 9, 1)
    row_lane = lax.broadcasted_iota(jnp.int32, (1, 128), 1)
    comb[...] = jnp.zeros_like(comb)
    for t in range(tok):
        total = back_recv[slot_of[t * top]].astype(F32)
        for k in range(1, top):
            total = total + back_recv[slot_of[t * top + k]].astype(F32)
        comb[t] = total
        s = slot_of[t * top + q]
        value = jnp.where(row_lane == s % cap, gp_recv[s // cap], 0.0)
        grow[t : t + 1, :] = value / jnp.full((1, 128), weight_of[t * top + q], F32)
    gr_out[...] = jnp.sum(grow[...], axis=1, keepdims=True)
    swap_tok = swap_matrix(nb, 16)
    for part_no in range(2):
        lo = part_no * 16
        hi = min(tok, lo + 16)
        v = comb[lo : lo + 16].reshape(16 * nb, 128)
        top_half = v.astype(BF16)
        rest = (v - top_half.astype(F32)).astype(BF16)
        moved = dot_nn(swap_tok, top_half) + dot_nn(swap_tok, rest)
        for b in range(nb):
            cols = slice(b * 128, (b + 1) * 128)
            value = moved[b * 16 : b * 16 + hi - lo]
            value = value + sdx_send[q, lo:hi, cols].astype(F32)
            for i in range(1, tp):
                value = value + sdx_recv[tp_peer(i), lo:hi, cols].astype(F32)
            dx_out[lo:hi, cols] = value.astype(BF16)

    waits(gw_out.at[:, :, 0 : (tp - 1) * dq], 10, 1)
    waits(wq.at[pl.ds(0, 3 * (tp - 1) * fo), :], 0, 0)
    waits(send_x.at[pl.ds(0, (ep - 1) * chunk), :], 1, 0)
    waits(sdx_send.at[pl.ds(0, tp - 1)], 2, 0)
    waits(sh1_recv, 3, 0)
    if ny > 1:
        waits(sh2.at[pl.ds(0, ny - 1)], 4, 0)
    if nz > 1:
        waits(sh3.at[pl.ds(0, nz - 1)], 5, 0)
    waits(rs_send.at[pl.ds(0, (tp - 1) * own_rows), :], 6, 0)
    waits(dall.at[pl.ds(0, (tp - 1) * own_rows), :], 7, 0)
    waits(back_send.at[pl.ds(0, (ep - 1) * cap)], 8, 0)
    waits(gp_send.at[pl.ds(0, ep - 1)], 9, 0)
    waits(dw_send.at[pl.ds(0, 3 * (tp - 1) * fo), :], 10, 0)
    waits(sh4, 11, 0)


def local(axes, cap, tokens, cotangent, routes, route_weights, expert_gate, expert_up, expert_down, shared_gate, shared_up, shared_down):
    tok, width = tokens.shape
    top = routes.shape[1]
    nz, ny, _ = axes
    ep = lax.axis_size("ep")
    tp = lax.axis_size("tp")
    fo = expert_gate.shape[2]
    ff = fo * tp
    dq = width // tp
    nb = dq // 128
    cb = width // (nz * ny)
    slots = ep * cap
    own_rows = slots // tp
    chunk = cap * 2 * nb
    wide = -(-(3 * ff + 1) // 128) * 128
    half = 3 * fo // 2

    flat = routes.reshape(-1)
    count = tok * top
    row = jnp.arange(count, dtype=jnp.int32) // top
    same = (flat[:, None] == flat[None, :]) & (row[None, :] < row[:, None])
    slot_of = flat * cap + jnp.sum(same.astype(jnp.int32), axis=1)
    hit = slot_of[None, :] == jnp.arange(slots, dtype=jnp.int32)[:, None]
    number = jnp.arange(count, dtype=jnp.int32) - count
    assign_of = count + jnp.sum(jnp.where(hit, number[None, :], 0), axis=1)
    weight_of = jnp.concatenate([route_weights.reshape(-1), jnp.zeros((8,), F32)])

    sizes = (ep, tp, nz, ny, cap, tok, top, dq, ff, cb)
    vmem = pl.BlockSpec(memory_space=pltpu.VMEM)
    smem = pl.BlockSpec(memory_space=pltpu.SMEM)
    dx, gr, gw, gs = pl.pallas_call(
        functools.partial(kernel, sizes),
        out_shape=(
            jax.ShapeDtypeStruct((tok, dq), BF16),
            jax.ShapeDtypeStruct((tok, 1), F32),
            jax.ShapeDtypeStruct((3, fo, width), BF16),
            jax.ShapeDtypeStruct((3 * fo, cb // 2), F32),
        ),
        in_specs=[smem] * 3 + [vmem] * 8,
        out_specs=(vmem,) * 4,
        scratch_shapes=[
            pltpu.VMEM((32, 2 * nb, 128), F32),
            pltpu.VMEM((slots * 2 * nb, 128), BF16),
            pltpu.VMEM((slots * 2 * nb, 128), BF16),
            pltpu.VMEM((3 * ff, dq), BF16),
            pltpu.VMEM((slots, 2 * dq), BF16),
            pltpu.VMEM((slots, wide), F32),
            pltpu.VMEM((slots, wide), BF16),
            pltpu.VMEM((slots, wide), BF16),
            pltpu.VMEM((slots, wide), BF16),
            pltpu.VMEM((slots, nb, 128), BF16),
            pltpu.VMEM((slots, nb, 128), BF16),
            pltpu.VMEM((ep, 1, 128), F32),
            pltpu.VMEM((ep, 1, 128), F32),
            pltpu.VMEM((3 * ff, dq), BF16),
            pltpu.VMEM((tp, tok, dq), BF16),
            pltpu.VMEM((tp, tok, dq), BF16),
            pltpu.VMEM((2, ny, nz, half, cb), BF16),
            pltpu.VMEM((ny, nz, half, cb), BF16),
            pltpu.VMEM((ny, nz, half, cb), BF16),
            pltpu.VMEM((ny, nz, half, cb), BF16),
            pltpu.VMEM((nz, half, cb), BF16),
            pltpu.VMEM((nz, half, cb), BF16),
            pltpu.VMEM((half, cb), F32),
            pltpu.VMEM((half, cb), F32),
            pltpu.VMEM((32, nb, 128), F32),
            pltpu.VMEM((tok, 128), F32),
            pltpu.SemaphoreType.DMA((24,)),
        ],
        compiler_params=pltpu.CompilerParams(
            collective_id=0, has_side_effects=True, vmem_limit_bytes=48 * 1024 * 1024
        ),
    )(
        assign_of,
        slot_of,
        weight_of,
        tokens,
        cotangent,
        expert_gate[0].T,
        expert_up[0].T,
        expert_down[0],
        shared_gate.T,
        shared_up.T,
        shared_down,
    )
    gw = gw.astype(F32)
    return (
        dx,
        gr,
        gw[0].T[None],
        gw[1].T[None],
        gw[2][None],
        gs[0:fo].T,
        gs[fo : 2 * fo].T,
        gs[2 * fo :],
    )


def solution(mesh):
    placed = (
        P("ep", None),
        P("ep", None),
        P("ep", None),
        P("ep", None),
        P("ep", None, "tp"),
        P("ep", None, "tp"),
        P("ep", "tp", None),
        P(None, "tp"),
        P(None, "tp"),
        P("tp", None),
    )
    return jax.shard_map(
        functools.partial(local, EP_AXES, CAP),
        mesh=mesh,
        in_specs=placed,
        out_specs=(
            P("ep", "tp"),
            P("ep", "tp"),
            P("ep", None, "tp"),
            P("ep", None, "tp"),
            P("ep", "tp", None),
            P("ep", "tp"),
            P("ep", "tp"),
            P("tp", "ep"),
        ),
        check_vma=False,
    )
```

time: 298 us -> 80.4 us (0.27)
  waiting for transfers between devices: 162 us -> 0 us
  Pallas kernels: 0 us -> 65.2 us
  starting transfers between devices: 37.1 us -> 0 us
  local copies, waits for them, and re-layouts: 48.6 us -> 13.5 us
  matrix products: 18.5 us -> 0 us
  between operations: 14.4 us -> 0.7 us
  blocking collectives: 9.19 us -> 0 us
  other arithmetic: 5.87 us -> 0.55 us
    all_to_all x5 -> x0, waiting for transfers between devices: 137 us -> none  [the longest x1 50 us: local(): lax.all_to_all(dx_sent.astype(jnp.bfloat16), 'ep', split_axis=0, concat_a...]
    pallas_call x0 -> x1, Pallas kernels: none -> 65.2 us  [local(): pl.pallas_call(functools.partial(kernel, sizes), out_shape=(jax.ShapeDtyp...]
    all_to_all x5 -> x0, starting transfers between devices: 37 us -> none  [the longest x1 13.2 us: local(): lax.all_to_all(send_w, 'ep', split_axis=0, concat_axis=0, tiled=True)]
    reduce_scatter x1 -> x0, waiting for transfers between devices: 23.5 us -> none  [local(): lax.psum_scatter((routed + shared_dx).astype(jnp.bfloat16), 'tp', scatter...]
    dot_general x16 -> x0, matrix products: 18.5 us -> none  [the longest x3 4.07 us: contract_cols(): lax.dot_general(left, right, (((1,), (1,)), ((), ())), preferred_element_...]
    reshape x5 -> x1, local copies, waits for them, and re-layouts: 11.3 us -> 0.09 us  [local(): flat = routes.reshape(-1)]
    gather x5 -> x0, local copies, waits for them, and re-layouts: 9.46 us -> none  [the longest x1 2.68 us: local(): send_g = padded_g[slot_token].reshape(all_experts, capacity, width)]
    unnamed x1 -> x0, blocking collectives: 9.19 us -> none
  transfers between devices with their start and end apart: 7 -> 0, of which waited for: 7 -> 0; matrix products, arithmetic and copies ran while one was open for 22% -> 0% of each run, Pallas kernels for 0% -> 0%
where the time goes in v1:
time: 80.4 us; the launch traced here: 80 us
  Pallas kernels  65.2 us (81%)
  local copies, waits for them, and re-layouts  13.5 us (17%)
    pallas_call x1, Pallas kernels, local(): pl.pallas_call(functools.partial(kernel, sizes), out_shape=(jax.ShapeDtyp...  65.2 us
    unnamed x20, local copies, waits for them, and re-layouts  10.5 us

profile of v1, /device:TPU:1, one launch (start us, length us, event | category | flops | bytes accessed | tf_op | source)
XLA Modules:
  0.0 80.0 jit_solution(11292921388261386299)
XLA Ops:
  0.6 0.8 copy.24
  1.4 0.1 reshape.62
  1.5 0.2 convert_reduce_fusion
  1.7 0.1 select_reduce_fusion
  1.8 0.8 copy.25
  2.6 0.1 reshape.63
  2.7 0.0 copy-start
  2.7 1.0 %copy-done = bf16[1,4096,48]{1,2,0:T(8,128)(2,1)S(1)} copy-done((bf16[1,4096,48]{1,2,0:T(8,128)(2,1)S(1)}, bf16[1,4096,48]{1,2,0:T(8,128)(2,1)}, u32[]{:S(2)}) %copy-start) | copy-done | bytes 393240
  3.7 0.0 copy-start.1
  3.7 1.0 %copy-done.1 = bf16[1,4096,48]{1,2,0:T(8,128)(2,1)S(1)} copy-done((bf16[1,4096,48]{1,2,0:T(8,128)(2,1)S(1)}, bf16[1,4096,48]{1,2,0:T(8,128)(2,1)}, u32[]{:S(2)}) %copy-start.1) | copy-done | bytes 393240
  4.7 0.0 copy-start.2
  4.7 1.0 %copy-done.2 = bf16[1,48,4096]{2,1,0:T(8,128)(2,1)S(1)} copy-done((bf16[1,48,4096]{2,1,0:T(8,128)(2,1)S(1)}, bf16[1,48,4096]{2,1,0:T(8,128)(2,1)}, u32[]{:S(2)}) %copy-start.2) | copy-done | bytes 393240
  5.7 0.0 copy-start.3
  5.7 1.0 %copy-done.3 = bf16[4096,48]{0,1:T(8,128)(2,1)S(1)} copy-done((bf16[4096,48]{0,1:T(8,128)(2,1)S(1)}, bf16[4096,48]{0,1:T(8,128)(2,1)}, u32[]{:S(2)}) %copy-start.3) | copy-done | bytes 393240
  6.7 0.0 copy-start.4
  6.7 1.0 %copy-done.4 = bf16[4096,48]{0,1:T(8,128)(2,1)S(1)} copy-done((bf16[4096,48]{0,1:T(8,128)(2,1)S(1)}, bf16[4096,48]{0,1:T(8,128)(2,1)}, u32[]{:S(2)}) %copy-start.4) | copy-done | bytes 393240
  7.7 0.0 copy-start.5
  7.7 1.0 %copy-done.5 = bf16[48,4096]{1,0:T(8,128)(2,1)S(1)} copy-done((bf16[48,4096]{1,0:T(8,128)(2,1)S(1)}, bf16[48,4096]{1,0:T(8,128)(2,1)}, u32[]{:S(2)}) %copy-start.5) | copy-done | bytes 393240
  8.7 0.0 copy-start.6
  8.7 0.9 %copy-done.6 = bf16[24,4096]{1,0:T(8,128)(2,1)S(1)} copy-done((bf16[24,4096]{1,0:T(8,128)(2,1)S(1)}, bf16[24,4096]{1,0:T(8,128)(2,1)}, u32[]{:S(2)}) %copy-start.6) | copy-done | bytes 196632
  9.6 0.0 copy-start.7
  9.6 0.9 %copy-done.7 = bf16[24,4096]{1,0:T(8,128)(2,1)S(1)} copy-done((bf16[24,4096]{1,0:T(8,128)(2,1)S(1)}, bf16[24,4096]{1,0:T(8,128)(2,1)}, u32[]{:S(2)}) %copy-start.7) | copy-done | bytes 196632
  10.5 65.2 %shard_map.161 = (bf16[24,1024]{1,0:T(8,128)(2,1)S(1)}, f32[24,1]{1,0:T(8,128)S(1)}, bf16[3,48,4096]{2,1,0:T(8,128)(2,1)S(1)}, f32[144,64]{1,0:T(8,128)S(1)}) custom-call(s32[192]{0:T(256)S(1)} %broadcast_add_fusion.assign_of, s32[96]{0:T(128)S(1)} %get-tuple-element.46.slot_of, f32[104]{0:T(128)S(1)} %concatenate.3.weight_of, ...), custom_call_target="tpu_custom_call" | custom-call | tf_op jit(solution)/shard_map/pallas_call | solution.py:398
  75.7 0.6 copy.26
  76.3 0.6 fusion
  77.0 0.9 %slice.26 = f32[1,48,4096]{2,1,0:T(8,128)} slice(bf16[3,48,4096]{2,1,0:T(8,128)(2,1)S(1)} %get-tuple-element.14), slice={[2:3], [0:48], [0:4096]} | slice | bytes 1572864 | tf_op jit(solution)/shard_map/slice | solution.py:459
  77.9 0.2 convert_element_type.7
  78.1 1.2 %slice_bitcast_fusion = (f32[1,4096,48]{1,2,0:T(8,128)}, f32[1,4096,48]{1,2,0:T(8,128)}) fusion(f32[3,48,4096]{2,1,0:T(8,128)S(1)} %convert_element_type.7), kind=kLoop, calls=%fused_computation | loop fusion | bytes 3145728 | tf_op jit(solution)/shard_map/broadcast_in_dim | solution.py:458
  79.4 0.6 copy.28
  (4 shorter events, 0.0 us)
Async XLA Ops:
  2.7 1.0 %copy-start = (bf16[1,4096,48]{1,2,0:T(8,128)(2,1)S(1)}, bf16[1,4096,48]{1,2,0:T(8,128)(2,1)}, u32[]{:S(2)}) copy-start(bf16[1,4096,48]{1,2,0:T(8,128)(2,1)} %param.14) | copy-start | bytes 1179652
  3.7 1.0 %copy-start.1 = (bf16[1,4096,48]{1,2,0:T(8,128)(2,1)S(1)}, bf16[1,4096,48]{1,2,0:T(8,128)(2,1)}, u32[]{:S(2)}) copy-start(bf16[1,4096,48]{1,2,0:T(8,128)(2,1)} %param.15) | copy-start | bytes 1179652
  4.7 1.0 %copy-start.2 = (bf16[1,48,4096]{2,1,0:T(8,128)(2,1)S(1)}, bf16[1,48,4096]{2,1,0:T(8,128)(2,1)}, u32[]{:S(2)}) copy-start(bf16[1,48,4096]{2,1,0:T(8,128)(2,1)} %param.16) | copy-start | bytes 1179652
  5.7 1.0 %copy-start.3 = (bf16[4096,48]{0,1:T(8,128)(2,1)S(1)}, bf16[4096,48]{0,1:T(8,128)(2,1)}, u32[]{:S(2)}) copy-start(bf16[4096,48]{0,1:T(8,128)(2,1)} %param.17) | copy-start | bytes 1179652
  6.7 1.0 %copy-start.4 = (bf16[4096,48]{0,1:T(8,128)(2,1)S(1)}, bf16[4096,48]{0,1:T(8,128)(2,1)}, u32[]{:S(2)}) copy-start(bf16[4096,48]{0,1:T(8,128)(2,1)} %param.18) | copy-start | bytes 1179652
  7.7 1.0 %copy-start.5 = (bf16[48,4096]{1,0:T(8,128)(2,1)S(1)}, bf16[48,4096]{1,0:T(8,128)(2,1)}, u32[]{:S(2)}) copy-start(bf16[48,4096]{1,0:T(8,128)(2,1)} %sd_ref.1) | copy-start | bytes 1179652
  8.7 0.9 %copy-start.6 = (bf16[24,4096]{1,0:T(8,128)(2,1)S(1)}, bf16[24,4096]{1,0:T(8,128)(2,1)}, u32[]{:S(2)}) copy-start(bf16[24,4096]{1,0:T(8,128)(2,1)} %x_ref.1) | copy-start | bytes 589828
  9.6 0.9 %copy-start.7 = (bf16[24,4096]{1,0:T(8,128)(2,1)S(1)}, bf16[24,4096]{1,0:T(8,128)(2,1)}, u32[]{:S(2)}) copy-start(bf16[24,4096]{1,0:T(8,128)(2,1)} %g_ref.1) | copy-start | bytes 589828

commit v2 on v1

v2 whole, which is shorter than its diff:
```python
import functools

import jax
import jax.numpy as jnp
from jax import lax
from jax.experimental import pallas as pl
from jax.experimental.pallas import tpu as pltpu
from jax.sharding import PartitionSpec as P

MESH = pl.DeviceIdType.MESH
F32 = jnp.float32
BF16 = jnp.bfloat16
I32 = jnp.int32
EP_AXES = (8, 4, 2)
CAP = 3
(WEIGHTS, DISPATCH, SHARED_DX, SHARED_1, SHARED_2, SHARED_3, SHARED_4, SCATTER, GATHER, BACK, GP, GRADS) = range(
    0, 72, 6
)


def dot_nn(a, b):
    return lax.dot_general(a, b, (((1,), (0,)), ((), ())), preferred_element_type=F32)


def dot_nt(a, b):
    return lax.dot_general(a, b, (((1,), (1,)), ((), ())), preferred_element_type=F32)


def dot_tn(a, b):
    return lax.dot_general(a, b, (((0,), (0,)), ((), ())), preferred_element_type=F32)


def wait_bytes(ref, sem):
    pltpu.make_async_copy(ref, ref, sem).wait()


def swish_parts(v):
    sigma = jax.nn.sigmoid(v)
    return v * sigma, sigma * (1.0 + v * (1.0 - sigma))


def swap_matrix(outer, inner):
    size = outer * inner
    row = lax.broadcasted_iota(I32, (size, size), 0)
    col = lax.broadcasted_iota(I32, (size, size), 1)
    return ((row % inner) * outer + row // inner == col).astype(BF16)


def z_order(nz):
    steps = sorted(range(1, nz), key=lambda dz: (-min(dz, nz - dz), dz))
    near = [dz for dz in steps if min(dz, nz - dz) <= 2]
    return tuple([dz for dz in steps if dz not in near] + [0] + near)


def groups_of(ep):
    return ((0, ep // 2), (ep // 2, ep // 4), (ep // 2 + ep // 4, ep // 4))


def kernel(
    sizes,
    routes_in,
    weights_in,
    x_in,
    g_in,
    wg_in,
    wu_in,
    wd_in,
    sg_in,
    su_in,
    sd_in,
    dx_out,
    gr_out,
    gg_out,
    gu_out,
    gd_out,
    gs_out,
    routes,
    weights,
    weight_turn,
    assign_table,
    assign_of,
    scale_table,
    scale_of,
    slot_table,
    slot_of,
    turn,
    x_ref,
    g_ref,
    sg_ref,
    su_ref,
    sd_ref,
    tiles,
    send_x,
    recv_x,
    wq,
    rows,
    part,
    rs_send,
    rs_recv,
    rest,
    rest_send,
    rest_recv,
    dall,
    dfull,
    back_send,
    back_recv,
    gp_send,
    gp_recv,
    dw_send,
    sdx_send,
    sdx_recv,
    sh1,
    sh1_recv,
    sh2,
    sh2_recv,
    sh3,
    sh3_recv,
    sh4,
    sh4_recv,
    comb,
    grow,
    gs_held,
    dx_held,
    gr_held,
    sem,
    in_sem,
):
    ep, tp, nz, ny, cap, tok, top, dq, ff, cb = sizes
    nb = dq // 128
    nyc = 2 * ny
    groups = groups_of(ep)
    first_rows = groups[0][1] * cap
    own_rows = first_rows // tp
    fo = ff // tp
    chunk = cap * 2 * nb
    me = lax.axis_index("ep")
    q = lax.axis_index("tp")
    core = lax.rem(me, 2)
    yc = lax.rem(me, nyc)
    yy = yc // 2
    zz = me // nyc
    sib = me + 1 - 2 * core

    def tp_peer(i):
        return lax.rem(q + i, tp)

    def to_of(dz, w):
        return lax.rem(zz + dz, nz) * nyc + lax.rem(yc + w, nyc)

    def from_of(dz, w):
        return lax.rem(zz + nz - dz, nz) * nyc + lax.rem(yc + nyc - w, nyc)

    def send(src, dst, kind, device):
        pltpu.make_async_remote_copy(
            src_ref=src,
            dst_ref=dst,
            send_sem=sem.at[kind],
            recv_sem=sem.at[kind + 1],
            device_id=device,
            device_id_type=MESH,
        ).start()

    def waits(ref, kind, side):
        wait_bytes(ref, sem.at[kind + side])

    def positions(group):
        start, count = groups[group]
        for k, dz in enumerate(z_order(nz)):
            lo = max(k * nyc, start)
            hi = min((k + 1) * nyc, start + count)
            if lo < hi:
                yield lo - k * nyc, hi - k * nyc, dz, k * nyc

    own_place = z_order(nz).index(0) * nyc

    def block_of(i, size):
        return pl.ds(pl.multiple_of(i * size, size), size)

    barrier = pltpu.get_barrier_semaphore()
    for dz in z_order(nz):

        @pl.loop(1 if dz == 0 else 0, nyc)
        def _(w):
            pl.semaphore_signal(barrier, inc=1, device_id={"ep": to_of(dz, w)}, device_id_type=MESH)

    for i in range(1, tp):
        pl.semaphore_signal(barrier, inc=1, device_id={"tp": tp_peer(i)}, device_id_type=MESH)

    own_cols = pl.ds(pl.multiple_of(q * dq, 128), dq)
    fetches = [
        pltpu.make_async_copy(src, dst, in_sem.at[n])
        for n, (src, dst) in enumerate(
            [
                (routes_in, routes),
                (weights_in, weights),
                (x_in, x_ref),
                (g_in, g_ref),
                (sg_in, sg_ref),
                (su_in, su_ref),
                (sd_in, sd_ref),
            ]
            + [
                (ref.at[:, own_cols], wq.at[pl.ds(pl.multiple_of(t * ff + q * fo, 16), fo), :])
                for t, ref in enumerate((wg_in, wu_in, wd_in))
            ]
        )
    ]
    for fetch in fetches:
        fetch.start()

    fetches[0].wait()
    turn[...] = jnp.zeros_like(turn)
    turn[0:top, 0:tok] = routes[...]
    by_row = turn[...].T
    fetches[1].wait()
    weight_turn[...] = jnp.zeros_like(weight_turn)
    weight_turn[0:top, 0:tok] = weights[...]
    weight_by_row = weight_turn[...].T
    expert = lax.broadcasted_iota(I32, (32, 128), 1)
    token = lax.broadcasted_iota(I32, (32, 128), 0)
    named = [(by_row[0:32, k : k + 1] == expert) & (token < tok) for k in range(top)]
    count = jnp.zeros((32, 128), I32)
    for k in range(top):
        count = count + named[k].astype(I32)
    before = count
    for shift in (1, 2, 4, 8, 16):
        before = before + jnp.where(token < shift, 0, pltpu.roll(before, shift, 0))
    before = before - count
    weight = jnp.zeros((32, 128), F32)
    for k in range(top):
        weight = weight + jnp.where(named[k], weight_by_row[0:32, k : k + 1], 0.0)
    slot = jnp.zeros((32, 128), I32)
    for k in range(top):
        mine = jnp.sum(jnp.where(named[k], expert * cap + before, 0), axis=1, keepdims=True)
        slot = jnp.where(expert == k, mine, slot)
    slot_table[...] = slot
    for j in range(cap):
        here = (count > 0) & (before == j)
        which = jnp.sum(jnp.where(here, token + 1, 0), axis=0, keepdims=True)
        assign_table[j : j + 1, :] = jnp.where(which > 0, which - 1, tok)
        scale_table[j : j + 1, :] = jnp.sum(jnp.where(here, weight, 0.0), axis=0, keepdims=True)
    tables = [
        pltpu.make_async_copy(assign_table, assign_of, in_sem.at[10]),
        pltpu.make_async_copy(scale_table, scale_of, in_sem.at[11]),
        pltpu.make_async_copy(slot_table, slot_of, in_sem.at[12]),
    ]
    for table in tables:
        table.start()

    fetches[2].wait()
    fetches[3].wait()
    col0 = q * dq
    swap_out = swap_matrix(16, 2 * nb)
    for part_no in range(2):
        lo = part_no * 16
        hi = min(tok, lo + 16)
        pieces = []
        for ref in (x_ref, g_ref):
            for b in range(nb):
                cols = pl.ds(pl.multiple_of(col0 + b * 128, 128), 128)
                piece = ref[lo:hi, cols].astype(F32)
                if hi - lo < 16:
                    piece = jnp.concatenate([piece, jnp.zeros((16 - hi + lo, 128), F32)], axis=0)
                pieces.append(piece)
        stacked = jnp.concatenate(pieces, axis=0).astype(BF16)
        moved = dot_nn(swap_out, stacked)
        tiles[lo : lo + 16] = moved.reshape(16, 2 * nb, 128)

    for table in tables:
        table.wait()
    lower = lax.broadcasted_iota(I32, (2 * nb, 128), 0) < nb

    @pl.loop(0, ep, unroll=4)
    def _(e):
        for j in range(cap):
            tile = tiles[assign_of[j, e]]
            scale = jnp.where(lower, jnp.float32(1.0), scale_of[j, e])
            at = pl.ds(pl.multiple_of((e * cap + j) * 2 * nb, 2 * nb), 2 * nb)
            send_x[at, :] = (tile * scale).astype(BF16)

    pl.semaphore_wait(barrier, ep - 1 + tp - 1)

    def dispatch(group):
        for lo, hi, dz, place in positions(group):

            @pl.loop(max(lo, 1) if dz == 0 else lo, hi)
            def _(w):
                p = to_of(dz, w)
                send(
                    send_x.at[block_of(p, chunk), :],
                    recv_x.at[block_of(place + w, chunk), :],
                    DISPATCH + 2 * group,
                    {"ep": p},
                )

    for t, ref in enumerate((wg_in, wu_in, wd_in)):
        for i in range(1, tp):
            dst_rows = pl.ds(pl.multiple_of(t * ff + q * fo, 16), fo)
            src_cols = pl.ds(pl.multiple_of(tp_peer(i) * dq, 128), dq)
            send(ref.at[:, src_cols], wq.at[dst_rows, :], WEIGHTS, {"tp": tp_peer(i)})
    dispatch(0)
    dispatch(1)
    dispatch(2)
    recv_x[own_place * chunk : (own_place + 1) * chunk, :] = send_x[block_of(me, chunk), :]

    for n in (4, 5, 6):
        fetches[n].wait()
    x = x_ref[...]
    s_gate = dot_nt(x, sg_ref[...])
    s_up = dot_nt(x, su_ref[...])
    s_back = dot_nt(g_ref[...], sd_ref[...])
    s_active, s_slope = swish_parts(s_gate)
    s_hidden = (s_active * s_up).astype(BF16)
    ds_gate = (s_back * s_up * s_slope).astype(BF16)
    ds_up = (s_back * s_active).astype(BF16)
    for j in range(tp):
        cols = slice(j * dq, (j + 1) * dq)
        piece = dot_nn(ds_gate, sg_ref[:, cols]) + dot_nn(ds_up, su_ref[:, cols])
        sdx_send[j] = piece.astype(BF16)
    for i in range(1, tp):
        send(sdx_send.at[tp_peer(i)], sdx_recv.at[q], SHARED_DX, {"tp": tp_peer(i)})

    half = 3 * fo // 2
    for z in range(nz):
        cols = slice(z * ny * cb, (z + 1) * ny * cb)
        xz = x_ref[:, cols]
        whole = jnp.concatenate(
            [dot_tn(ds_gate, xz), dot_tn(ds_up, xz), dot_tn(s_hidden, g_ref[:, cols])], axis=0
        )
        for y in range(ny):
            for h in range(2):
                sh1[h, y, z] = whole[h * half : (h + 1) * half, y * cb : (y + 1) * cb].astype(BF16)
    send(sh1.at[1 - core], sh1_recv, SHARED_1, {"ep": sib})

    waits(sh1_recv, SHARED_1, 1)
    for y in range(ny):
        for z in range(nz):
            both = sh1[core, y, z].astype(F32) + sh1_recv[y, z].astype(F32)
            sh2[y, z] = both.astype(BF16)
    for i in range(1, ny):
        y = lax.rem(yy + i, ny)
        send(sh2.at[y], sh2_recv.at[yy], SHARED_2, {"ep": (zz * ny + y) * 2 + core})

    swap_in = swap_matrix(2 * nb, 16)
    swap_back = swap_matrix(16, nb)

    def arrived(group):
        start, count = groups[group]
        own = 1 if start <= own_place < start + count else 0
        waits(recv_x.at[pl.ds(0, (count - own) * chunk), :], DISPATCH + 2 * group, 1)

    def contract(group):
        base, count = groups[group][0] * cap, groups[group][1] * cap
        for n in range(count // 16):
            lo = base + n * 16
            moved = dot_nn(swap_in, recv_x[lo * 2 * nb : (lo + 16) * 2 * nb, :]).astype(BF16)
            for b in range(2 * nb):
                rows[lo : lo + 16, b * 128 : (b + 1) * 128] = moved[b * 16 : (b + 1) * 16]
        up_part = dot_nt(rows[base : base + count, 0:dq], wq[0 : 2 * ff, :])
        back_part = dot_nt(rows[base : base + count, dq : 2 * dq], wq[2 * ff : 3 * ff, :])
        return up_part, back_part

    def scatter_first():
        up_part, back_part = contract(0)
        for b in range(tp):
            here = slice(b * own_rows, (b + 1) * own_rows)
            part[b, :, 0 : 2 * ff] = up_part[here]
            part[b, :, 2 * ff : 3 * ff] = back_part[here]
            rs_send[b, :, 0 : 2 * ff] = up_part[here].astype(BF16)
            rs_send[b, :, 2 * ff : 3 * ff] = back_part[here].astype(BF16)
        for i in range(1, tp):
            send(rs_send.at[tp_peer(i)], rs_recv.at[q], SCATTER, {"tp": tp_peer(i)})

    def spread_rest(group):
        up_part, back_part = contract(group)
        n = group - 1
        rest[n, :, 0 : 2 * ff] = up_part
        rest[n, :, 2 * ff : 3 * ff] = back_part
        rest_send[n, :, 0 : 2 * ff] = up_part.astype(BF16)
        rest_send[n, :, 2 * ff : 3 * ff] = back_part.astype(BF16)
        for i in range(1, tp):
            send(rest_send.at[n], rest_recv.at[n, q], SCATTER + 2 * group, {"tp": tp_peer(i)})

    def gradients(total):
        gate = total[:, 0:ff]
        up = total[:, ff : 2 * ff]
        back = total[:, 2 * ff : 3 * ff]
        active, slope = swish_parts(gate)
        hidden = (active * up).astype(BF16).astype(F32)
        gp = jnp.sum(hidden * back, axis=1, keepdims=True)
        extra = dfull.shape[1] - 3 * ff
        return jnp.concatenate(
            [back * up * slope, back * active, hidden, jnp.broadcast_to(gp, (gp.shape[0], extra))], axis=1
        )

    def gather_first():
        waits(rs_recv.at[pl.ds(0, tp - 1)], SCATTER, 1)
        total = part[q]
        for i in range(1, tp):
            total = total + rs_recv[tp_peer(i)].astype(F32)
        dall[q] = gradients(total).astype(BF16)
        mine = dall.at[q]
        for i in range(1, tp):
            send(mine, mine, GATHER, {"tp": tp_peer(i)})

    def finish_first():
        waits(dall.at[pl.ds(0, tp - 1)], GATHER, 1)
        for b in range(tp):
            dfull[b * own_rows : (b + 1) * own_rows, :] = dall[b].astype(F32)

    def finish_rest(group):
        n = group - 1
        waits(rest_recv.at[n, pl.ds(0, tp - 1)], SCATTER + 2 * group, 1)
        total = rest[n]
        for i in range(1, tp):
            total = total + rest_recv[n, tp_peer(i)].astype(F32)
        base, count = groups[group][0] * cap, groups[group][1] * cap
        dfull[base : base + count, :] = gradients(total)

    def send_back(group):
        start, places = groups[group]
        base, count = start * cap, places * cap
        d = dfull[base : base + count, :]
        dxr = dot_nn(d[:, 0 : 2 * ff].astype(BF16), wq[0 : 2 * ff, :])
        for n in range(count // 16):
            stacked = jnp.concatenate(
                [dxr[n * 16 : (n + 1) * 16, b * 128 : (b + 1) * 128] for b in range(nb)], axis=0
            ).astype(BF16)
            moved = dot_nn(swap_back, stacked)
            back_send[base + n * 16 : base + (n + 1) * 16] = moved.reshape(16, nb, 128).astype(BF16)
        src_row = lax.broadcasted_iota(I32, (places, count), 0)
        src_col = lax.broadcasted_iota(I32, (places, count), 1)
        collect = (src_col // cap == src_row).astype(F32)
        lane = lax.broadcasted_iota(I32, (count, 128), 1)
        slot_row = lax.broadcasted_iota(I32, (count, 128), 0)
        spread = jnp.where(lane == slot_row % cap, d[:, 3 * ff : 3 * ff + 1], 0.0)
        gp_send[start : start + places] = dot_nn(collect, spread).reshape(places, 1, 128)
        for lo, hi, dz, place in positions(group):
            if dz == 0 and lo == 0:
                back_recv[pl.ds(me * cap, cap)] = back_send[place * cap : (place + 1) * cap]
                gp_recv[me] = gp_send[place]

            @pl.loop(max(lo, 1) if dz == 0 else lo, hi)
            def _(w):
                to = {"ep": from_of(dz, w)}
                send(
                    back_send.at[pl.ds((place + w) * cap, cap)],
                    back_recv.at[pl.ds(me * cap, cap)],
                    BACK,
                    to,
                )
                send(gp_send.at[place + w], gp_recv.at[me], GP, to)

    arrived(0)
    for n in (7, 8, 9):
        fetches[n].wait()
    waits(wq.at[pl.ds(0, 3 * (tp - 1) * fo), :], WEIGHTS, 1)
    scatter_first()
    arrived(1)
    spread_rest(1)
    gather_first()
    arrived(2)
    spread_rest(2)
    if ny > 1:
        waits(sh2_recv.at[pl.ds(0, ny - 1)], SHARED_2, 1)
    for z in range(nz):
        total = sh2[yy, z].astype(F32)
        for i in range(1, ny):
            total = total + sh2_recv[lax.rem(yy + i, ny), z].astype(F32)
        sh3[z] = total.astype(BF16)
    for i in range(1, nz):
        z = lax.rem(zz + i, nz)
        send(sh3.at[z], sh3_recv.at[zz], SHARED_3, {"ep": (z * ny + yy) * 2 + core})
    finish_first()
    send_back(0)
    finish_rest(1)
    send_back(1)
    finish_rest(2)
    d = dfull[...].astype(BF16)
    dw_send[0 : 2 * ff, :] = dot_tn(d[:, 0 : 2 * ff], rows[:, 0:dq]).astype(BF16)
    dw_send[2 * ff : 3 * ff, :] = dot_tn(d[:, 2 * ff : 3 * ff], rows[:, dq : 2 * dq]).astype(BF16)
    own_grads = []
    for t, out in enumerate((gg_out, gu_out, gd_out)):
        for i in range(1, tp):
            src_rows = pl.ds(pl.multiple_of(t * ff + tp_peer(i) * fo, 16), fo)
            send(dw_send.at[src_rows, :], out.at[:, own_cols], GRADS, {"tp": tp_peer(i)})
        mine = pl.ds(pl.multiple_of(t * ff + q * fo, 16), fo)
        own_grads.append(pltpu.make_async_copy(dw_send.at[mine, :], out.at[:, own_cols], in_sem.at[t]))
        own_grads[-1].start()
    send_back(2)

    if nz > 1:
        waits(sh3_recv.at[pl.ds(0, nz - 1)], SHARED_3, 1)
    total = sh3[zz].astype(F32)
    for i in range(1, nz):
        total = total + sh3_recv[lax.rem(zz + i, nz)].astype(F32)
    sh4[...] = total
    send(sh4, sh4_recv, SHARED_4, {"ep": sib})
    waits(sdx_recv.at[pl.ds(0, tp - 1)], SHARED_DX, 1)
    waits(sh4_recv, SHARED_4, 1)
    first = core == 0
    full = jnp.concatenate(
        [
            jnp.where(first, sh4[...], sh4_recv[...]),
            jnp.where(first, sh4_recv[...], sh4[...]),
        ],
        axis=0,
    )
    gs_held[...] = jnp.where(first, full[:, 0 : cb // 2], full[:, cb // 2 : cb])
    own_grads.append(pltpu.make_async_copy(gs_held, gs_out, in_sem.at[3]))
    own_grads[-1].start()

    waits(back_recv.at[pl.ds(0, (ep - 1) * cap)], BACK, 1)
    waits(gp_recv.at[pl.ds(0, ep - 1)], GP, 1)
    row_lane = lax.broadcasted_iota(I32, (1, 128), 1)
    comb[...] = jnp.zeros_like(comb)
    for t in range(tok):
        total = back_recv[slot_of[t, 0]].astype(F32)
        for k in range(1, top):
            total = total + back_recv[slot_of[t, k]].astype(F32)
        comb[t] = total
        s = slot_of[t, q]
        value = jnp.where(row_lane == s % cap, gp_recv[s // cap], 0.0)
        grow[t : t + 1, :] = value
    gr_held[...] = jnp.sum(grow[...].T, axis=0, keepdims=True)[:, 0:tok] / weights[pl.ds(q, 1), :]
    swap_tok = swap_matrix(nb, 16)
    for part_no in range(2):
        lo = part_no * 16
        hi = min(tok, lo + 16)
        v = comb[lo : lo + 16].reshape(16 * nb, 128)
        top_half = v.astype(BF16)
        rest = (v - top_half.astype(F32)).astype(BF16)
        moved = dot_nn(swap_tok, top_half) + dot_nn(swap_tok, rest)
        for b in range(nb):
            cols = slice(b * 128, (b + 1) * 128)
            value = moved[b * 16 : b * 16 + hi - lo]
            value = value + sdx_send[q, lo:hi, cols].astype(F32)
            for i in range(1, tp):
                value = value + sdx_recv[tp_peer(i), lo:hi, cols].astype(F32)
            dx_held[lo:hi, cols] = value.astype(BF16)

    for n, (src, dst) in enumerate(((dx_held, dx_out), (gr_held, gr_out))):
        own_grads.append(pltpu.make_async_copy(src, dst, in_sem.at[4 + n]))
        own_grads[-1].start()
    waits(wq.at[pl.ds(0, 3 * (tp - 1) * fo), :], WEIGHTS, 0)
    for group, (start, count) in enumerate(groups):
        own = 1 if start <= own_place < start + count else 0
        waits(send_x.at[pl.ds(0, (count - own) * chunk), :], DISPATCH + 2 * group, 0)
    waits(sdx_send.at[pl.ds(0, tp - 1)], SHARED_DX, 0)
    waits(sh1_recv, SHARED_1, 0)
    if ny > 1:
        waits(sh2.at[pl.ds(0, ny - 1)], SHARED_2, 0)
    if nz > 1:
        waits(sh3.at[pl.ds(0, nz - 1)], SHARED_3, 0)
    waits(rs_send.at[pl.ds(0, tp - 1)], SCATTER, 0)
    waits(dall.at[pl.ds(0, tp - 1)], GATHER, 0)
    for n in range(2):
        waits(rest_recv.at[n, pl.ds(0, tp - 1)], SCATTER + 2 + 2 * n, 0)
    waits(back_send.at[pl.ds(0, (ep - 1) * cap)], BACK, 0)
    waits(gp_send.at[pl.ds(0, ep - 1)], GP, 0)
    waits(sh4, SHARED_4, 0)
    waits(dw_send.at[pl.ds(0, 3 * (tp - 1) * fo), :], GRADS, 0)
    for copy in own_grads:
        copy.wait()
    waits(dw_send.at[pl.ds(0, 3 * (tp - 1) * fo), :], GRADS, 1)


def finish(fo, dx, gr, gg, gu, gd, gs, dx_o, gr_o, gg_o, gu_o, gd_o, gsg_o, gsu_o, gsd_o, narrow, wide, small, sem):
    width = gg.shape[1]
    parts = 2
    step = width // parts
    loads = []
    for t, src in enumerate((gg, gu, gd)):
        for c in range(parts):
            cols = slice(c * step, (c + 1) * step)
            loads.append(pltpu.make_async_copy(src.at[:, cols], narrow.at[t, :, cols], sem.at[t * parts + c]))
            loads[-1].start()
    last = 6 * parts
    others = [(gs, small[0]), (dx, small[1]), (gr, small[2])]
    ins = [pltpu.make_async_copy(src, dst, sem.at[last + n]) for n, (src, dst) in enumerate(others)]
    for copy in ins:
        copy.start()
    stores = []
    for t, dst in enumerate((gg_o, gu_o, gd_o)):
        for c in range(parts):
            cols = slice(c * step, (c + 1) * step)
            loads[t * parts + c].wait()
            wide[t, :, cols] = narrow[t, :, cols].astype(F32)
            stores.append(pltpu.make_async_copy(wide.at[t, :, cols], dst.at[:, cols], sem.at[(3 + t) * parts + c]))
            stores[-1].start()
    for copy in ins:
        copy.wait()
    outs = [(small[0].at[t * fo : (t + 1) * fo], dst) for t, dst in enumerate((gsg_o, gsu_o, gsd_o))]
    outs += [(small[1], dx_o), (small[2], gr_o)]
    for n, (src, dst) in enumerate(outs):
        stores.append(pltpu.make_async_copy(src, dst, sem.at[last + 3 + n]))
        stores[-1].start()
    for copy in stores:
        copy.wait()


def local(axes, cap, tokens, cotangent, routes, route_weights, expert_gate, expert_up, expert_down, shared_gate, shared_up, shared_down):
    tok, width = tokens.shape
    top = routes.shape[1]
    nz, ny, _ = axes
    ep = lax.axis_size("ep")
    tp = lax.axis_size("tp")
    fo = expert_gate.shape[2]
    ff = fo * tp
    dq = width // tp
    nb = dq // 128
    cb = width // (nz * ny)
    slots = ep * cap
    own_rows = slots // tp // 2
    wide = -(-(3 * ff + 1) // 128) * 128
    half = 3 * fo // 2

    sizes = (ep, tp, nz, ny, cap, tok, top, dq, ff, cb)
    vmem = pl.BlockSpec(memory_space=pltpu.VMEM)
    hbm = pl.BlockSpec(memory_space=pltpu.HBM)
    outs = pl.pallas_call(
        functools.partial(kernel, sizes),
        out_shape=(
            jax.ShapeDtypeStruct((tok, dq), BF16),
            jax.ShapeDtypeStruct((1, tok), F32),
            jax.ShapeDtypeStruct((fo, width), BF16),
            jax.ShapeDtypeStruct((fo, width), BF16),
            jax.ShapeDtypeStruct((fo, width), BF16),
            jax.ShapeDtypeStruct((3 * fo, cb // 2), F32),
        ),
        in_specs=[hbm] * 10,
        out_specs=(hbm,) * 6,
        scratch_shapes=[
            pltpu.VMEM((top, tok), I32),
            pltpu.VMEM((top, tok), F32),
            pltpu.VMEM((8, 128), F32),
            pltpu.VMEM((-(-cap // 8) * 8, 128), I32),
            pltpu.SMEM((-(-cap // 8) * 8, 128), I32),
            pltpu.VMEM((-(-cap // 8) * 8, 128), F32),
            pltpu.SMEM((-(-cap // 8) * 8, 128), F32),
            pltpu.VMEM((32, 128), I32),
            pltpu.SMEM((32, 128), I32),
            pltpu.VMEM((8, 128), I32),
            pltpu.VMEM((tok, width), BF16),
            pltpu.VMEM((tok, width), BF16),
            pltpu.VMEM((fo, width), BF16),
            pltpu.VMEM((fo, width), BF16),
            pltpu.VMEM((fo, width), BF16),
            pltpu.VMEM((32, 2 * nb, 128), F32),
            pltpu.VMEM((slots * 2 * nb, 128), BF16),
            pltpu.VMEM((slots * 2 * nb, 128), BF16),
            pltpu.VMEM((3 * ff, dq), BF16),
            pltpu.VMEM((slots, 2 * dq), BF16),
            pltpu.VMEM((tp, own_rows, 3 * ff), F32),
            pltpu.VMEM((tp, own_rows, 3 * ff), BF16),
            pltpu.VMEM((tp, own_rows, 3 * ff), BF16),
            pltpu.VMEM((2, slots // 4, 3 * ff), F32),
            pltpu.VMEM((2, slots // 4, 3 * ff), BF16),
            pltpu.VMEM((2, tp, slots // 4, 3 * ff), BF16),
            pltpu.VMEM((tp, own_rows, wide), BF16),
            pltpu.VMEM((slots, wide), F32),
            pltpu.VMEM((slots, nb, 128), BF16),
            pltpu.VMEM((slots, nb, 128), BF16),
            pltpu.VMEM((ep, 1, 128), F32),
            pltpu.VMEM((ep, 1, 128), F32),
            pltpu.VMEM((3 * ff, dq), BF16),
            pltpu.VMEM((tp, tok, dq), BF16),
            pltpu.VMEM((tp, tok, dq), BF16),
            pltpu.VMEM((2, ny, nz, half, cb), BF16),
            pltpu.VMEM((ny, nz, half, cb), BF16),
            pltpu.VMEM((ny, nz, half, cb), BF16),
            pltpu.VMEM((ny, nz, half, cb), BF16),
            pltpu.VMEM((nz, half, cb), BF16),
            pltpu.VMEM((nz, half, cb), BF16),
            pltpu.VMEM((half, cb), F32),
            pltpu.VMEM((half, cb), F32),
            pltpu.VMEM((32, nb, 128), F32),
            pltpu.VMEM((32, 128), F32),
            pltpu.VMEM((3 * fo, cb // 2), F32),
            pltpu.VMEM((tok, dq), BF16),
            pltpu.VMEM((1, tok), F32),
            pltpu.SemaphoreType.DMA((72,)),
            pltpu.SemaphoreType.DMA((13,)),
        ],
        compiler_params=pltpu.CompilerParams(
            collective_id=0, has_side_effects=True, vmem_limit_bytes=67043328
        ),
    )(
        routes.T,
        route_weights.T,
        tokens,
        cotangent,
        expert_gate[0].T,
        expert_up[0].T,
        expert_down[0],
        shared_gate.T,
        shared_up.T,
        shared_down,
    )
    dx, gr, gg, gu, gd, gsg, gsu, gsd = pl.pallas_call(
        functools.partial(finish, fo),
        out_shape=(
            jax.ShapeDtypeStruct((tok, dq), BF16),
            jax.ShapeDtypeStruct((1, tok), F32),
            jax.ShapeDtypeStruct((fo, width), F32),
            jax.ShapeDtypeStruct((fo, width), F32),
            jax.ShapeDtypeStruct((fo, width), F32),
            jax.ShapeDtypeStruct((fo, cb // 2), F32),
            jax.ShapeDtypeStruct((fo, cb // 2), F32),
            jax.ShapeDtypeStruct((fo, cb // 2), F32),
        ),
        in_specs=[hbm] * 6,
        out_specs=(hbm,) * 8,
        scratch_shapes=[
            pltpu.VMEM((3, fo, width), BF16),
            pltpu.VMEM((3, fo, width), F32),
            [pltpu.VMEM((3 * fo, cb // 2), F32), pltpu.VMEM((tok, dq), BF16), pltpu.VMEM((1, tok), F32)],
            pltpu.SemaphoreType.DMA((20,)),
        ],
        compiler_params=pltpu.CompilerParams(vmem_limit_bytes=67043328),
    )(*outs)
    return (dx, gr.T, gg.T[None], gu.T[None], gd[None], gsg.T, gsu.T, gsd)


def solution(mesh):
    placed = (
        P("ep", None),
        P("ep", None),
        P("ep", None),
        P("ep", None),
        P("ep", None, "tp"),
        P("ep", None, "tp"),
        P("ep", "tp", None),
        P(None, "tp"),
        P(None, "tp"),
        P("tp", None),
    )
    return jax.shard_map(
        functools.partial(local, EP_AXES, CAP),
        mesh=mesh,
        in_specs=placed,
        out_specs=(
            P("ep", "tp"),
            P("ep", "tp"),
            P("ep", None, "tp"),
            P("ep", None, "tp"),
            P("ep", "tp", None),
            P("ep", "tp"),
            P("ep", "tp"),
            P("tp", "ep"),
        ),
        check_vma=False,
    )
```

time: 80.4 us -> 61 us (0.76)
  local copies, waits for them, and re-layouts: 13.5 us -> 0 us
  Pallas kernels: 65.2 us -> 60.2 us
    unnamed x20 -> x0, local copies, waits for them, and re-layouts: 10.5 us -> none
    pallas_call x1, Pallas kernels: 65.2 us -> 57.7 us  [local(): pl.pallas_call(functools.partial(kernel, sizes), out_shape=(jax.ShapeDtyp...]
    pallas_call x0 -> x1, Pallas kernels: none -> 2.55 us  [local(): pl.pallas_call(functools.partial(finish, fo), out_shape=(jax.ShapeDtypeSt...]
    slice x2 -> x0, local copies, waits for them, and re-layouts: 1.56 us -> none  [the longest x1 0.93 us: local(): gw[2][None]]
    broadcast_in_dim x1 -> x0, local copies, waits for them, and re-layouts: 1.25 us -> none  [local(): gw[1].T[None]]
where the time goes in v2:
time: 61 us; the launch traced here: 60.9 us
  Pallas kernels  60.2 us (99%)
  between operations  0.64 us (1%)
    pallas_call x1, Pallas kernels, local(): pl.pallas_call(functools.partial(kernel, sizes), out_shape=(jax.ShapeDtyp...  57.7 us
    pallas_call x1, Pallas kernels, local(): pl.pallas_call(functools.partial(finish, fo), out_shape=(jax.ShapeDtypeSt...  2.55 us

profile of v2, /device:TPU:1, one launch (start us, length us, event | category | flops | bytes accessed | tf_op | source)
XLA Modules:
  0.0 60.9 jit_solution(13940734415762238429)
XLA Ops:
  0.6 57.7 %shard_map.161 = (bf16[24,1024]{1,0:T(8,128)(2,1)}, f32[1,24]{1,0:T(1,128)}, bf16[48,4096]{1,0:T(8,128)(2,1)}, bf16[48,4096]{1,0:T(8,128)(2,1)}, bf16[48,4096]{1,0:T(8,128)(2,1)}, /*index=5*/f32[144,64]{1,0:T(8,128)}) custom-call(s32[4,24]{1,0:T(4,128)} %bitcast.26, f32[4,24]{1,0:T(4,128)} %bitcast.27, bf16[24,4096]{1,0:T(8,128)(2,1)} %x_in.1, ...), custom_call_target="tpu_custom_call" | custom-call | tf_op jit(solution)/shard_map/pallas_call | solution.py:621
  58.3 2.6 %shard_map.162 = (bf16[24,1024]{1,0:T(8,128)(2,1)}, f32[1,24]{1,0:T(1,128)}, f32[48,4096]{1,0:T(8,128)}, f32[48,4096]{1,0:T(8,128)}, f32[48,4096]{1,0:T(8,128)},...) custom-call(bf16[24,1024]{1,0:T(8,128)(2,1)} %get-tuple-element.22.dx, f32[1,24]{1,0:T(1,128)} %get-tuple-element.23.gr, ...), custom_call_target="tpu_custom_call" | custom-call | tf_op jit(solution)/shard_map/pallas_call | solution.py:700

commit v3 on v2

--- a/solution.py
+++ b/solution.py
@@ -47,9 +47,9 @@
 
 
 def z_order(nz):
-    steps = sorted(range(1, nz), key=lambda dz: (-min(dz, nz - dz), dz))
-    near = [dz for dz in steps if min(dz, nz - dz) <= 2]
-    return tuple([dz for dz in steps if dz not in near] + [0] + near)
+    if nz == 8:
+        return (3, 5, 1, 7, 4, 0, 2, 6)
+    return tuple(range(nz))
 
 
 def groups_of(ep):
@@ -105,6 +105,7 @@
     back_send,
     back_recv,
     gp_send,
+    gp_mid,
     gp_recv,
     dw_send,
     sdx_send,
@@ -177,10 +178,8 @@
         return pl.ds(pl.multiple_of(i * size, size), size)
 
     barrier = pltpu.get_barrier_semaphore()
-    for dz in z_order(nz):
-
-        @pl.loop(1 if dz == 0 else 0, nyc)
-        def _(w):
+    for dz in sorted(range(nz), key=lambda dz: -min(dz, nz - dz)):
+        for w in range(1 if dz == 0 else 0, nyc):
             pl.semaphore_signal(barrier, inc=1, device_id={"ep": to_of(dz, w)}, device_id_type=MESH)
 
     for i in range(1, tp):
@@ -270,28 +269,28 @@
         table.wait()
     lower = lax.broadcasted_iota(I32, (2 * nb, 128), 0) < nb
 
-    @pl.loop(0, ep, unroll=4)
-    def _(e):
-        for j in range(cap):
-            tile = tiles[assign_of[j, e]]
-            scale = jnp.where(lower, jnp.float32(1.0), scale_of[j, e])
-            at = pl.ds(pl.multiple_of((e * cap + j) * 2 * nb, 2 * nb), 2 * nb)
-            send_x[at, :] = (tile * scale).astype(BF16)
-
-    pl.semaphore_wait(barrier, ep - 1 + tp - 1)
+    def pick(group):
+        for lo, hi, dz, place in positions(group):
+
+            @pl.loop(lo, hi, unroll=4)
+            def _(w):
+                p = to_of(dz, w)
+                for j in range(cap):
+                    tile = tiles[assign_of[j, p]]
+                    scale = jnp.where(lower, jnp.float32(1.0), scale_of[j, p])
+                    at = pl.ds(pl.multiple_of(((place + w) * cap + j) * 2 * nb, 2 * nb), 2 * nb)
+                    send_x[at, :] = (tile * scale).astype(BF16)
 
     def dispatch(group):
         for lo, hi, dz, place in positions(group):
 
-            @pl.loop(max(lo, 1) if dz == 0 else lo, hi)
+            @pl.loop(max(lo, 1) if dz == 0 else lo, hi, unroll=4)
             def _(w):
-                p = to_of(dz, w)
-                send(
-                    send_x.at[block_of(p, chunk), :],
-                    recv_x.at[block_of(place + w, chunk), :],
-                    DISPATCH + 2 * group,
-                    {"ep": p},
-                )
+                here = block_of(place + w, chunk)
+                send(send_x.at[here, :], recv_x.at[here, :], DISPATCH + 2 * group, {"ep": to_of(dz, w)})
+
+    pick(0)
+    pl.semaphore_wait(barrier, ep - 1 + tp - 1)
 
     for t, ref in enumerate((wg_in, wu_in, wd_in)):
         for i in range(1, tp):
@@ -299,9 +298,11 @@
             src_cols = pl.ds(pl.multiple_of(tp_peer(i) * dq, 128), dq)
             send(ref.at[:, src_cols], wq.at[dst_rows, :], WEIGHTS, {"tp": tp_peer(i)})
     dispatch(0)
+    pick(1)
     dispatch(1)
+    pick(2)
     dispatch(2)
-    recv_x[own_place * chunk : (own_place + 1) * chunk, :] = send_x[block_of(me, chunk), :]
+    recv_x[own_place * chunk : (own_place + 1) * chunk, :] = send_x[own_place * chunk : (own_place + 1) * chunk, :]
 
     for n in (4, 5, 6):
         fetches[n].wait()
@@ -317,9 +318,6 @@
         cols = slice(j * dq, (j + 1) * dq)
         piece = dot_nn(ds_gate, sg_ref[:, cols]) + dot_nn(ds_up, su_ref[:, cols])
         sdx_send[j] = piece.astype(BF16)
-    for i in range(1, tp):
-        send(sdx_send.at[tp_peer(i)], sdx_recv.at[q], SHARED_DX, {"tp": tp_peer(i)})
-
     half = 3 * fo // 2
     for z in range(nz):
         cols = slice(z * ny * cb, (z + 1) * ny * cb)
@@ -428,6 +426,24 @@
             ).astype(BF16)
             moved = dot_nn(swap_back, stacked)
             back_send[base + n * 16 : base + (n + 1) * 16] = moved.reshape(16, nb, 128).astype(BF16)
+        for lo, hi, dz, place in positions(group):
+            if dz == 0 and lo == 0:
+                back_recv[pl.ds(me * cap, cap)] = back_send[place * cap : (place + 1) * cap]
+
+            @pl.loop(max(lo, 1) if dz == 0 else lo, hi, unroll=4)
+            def _(w):
+                to = {"ep": from_of(dz, w)}
+                send(
+                    back_send.at[pl.ds((place + w) * cap, cap)],
+                    back_recv.at[pl.ds(me * cap, cap)],
+                    BACK,
+                    to,
+                )
+
+    def send_route_sums(group):
+        start, places = groups[group]
+        base, count = start * cap, places * cap
+        d = dfull[base : base + count, :]
         src_row = lax.broadcasted_iota(I32, (places, count), 0)
         src_col = lax.broadcasted_iota(I32, (places, count), 1)
         collect = (src_col // cap == src_row).astype(F32)
@@ -436,31 +452,35 @@
         spread = jnp.where(lane == slot_row % cap, d[:, 3 * ff : 3 * ff + 1], 0.0)
         gp_send[start : start + places] = dot_nn(collect, spread).reshape(places, 1, 128)
         for lo, hi, dz, place in positions(group):
-            if dz == 0 and lo == 0:
-                back_recv[pl.ds(me * cap, cap)] = back_send[place * cap : (place + 1) * cap]
-                gp_recv[me] = gp_send[place]
-
-            @pl.loop(max(lo, 1) if dz == 0 else lo, hi)
-            def _(w):
-                to = {"ep": from_of(dz, w)}
+            if dz == 0:
+                gp_mid[zz, lo:hi] = gp_send[place + lo : place + hi]
+            else:
                 send(
-                    back_send.at[pl.ds((place + w) * cap, cap)],
-                    back_recv.at[pl.ds(me * cap, cap)],
-                    BACK,
-                    to,
+                    gp_send.at[pl.ds(place + lo, hi - lo)],
+                    gp_mid.at[zz, pl.ds(lo, hi - lo)],
+                    GP,
+                    {"ep": from_of(dz, 0)},
                 )
-                send(gp_send.at[place + w], gp_recv.at[me], GP, to)
+
+    def spread_route_sums():
+        if nz > 1:
+            waits(gp_mid.at[pl.ds(0, nz - 1)], GP, 1)
+        for w in range(1, nyc):
+            send(gp_mid.at[:, w], gp_recv.at[:, yc], GP + 2, {"ep": from_of(0, w)})
+        gp_recv[:, yc] = gp_mid[:, 0]
 
     arrived(0)
     for n in (7, 8, 9):
         fetches[n].wait()
     waits(wq.at[pl.ds(0, 3 * (tp - 1) * fo), :], WEIGHTS, 1)
     scatter_first()
+    gather_first()
     arrived(1)
     spread_rest(1)
-    gather_first()
     arrived(2)
     spread_rest(2)
+    for i in range(1, tp):
+        send(sdx_send.at[tp_peer(i)], sdx_recv.at[q], SHARED_DX, {"tp": tp_peer(i)})
     if ny > 1:
         waits(sh2_recv.at[pl.ds(0, ny - 1)], SHARED_2, 1)
     for z in range(nz):
@@ -473,8 +493,8 @@
         send(sh3.at[z], sh3_recv.at[zz], SHARED_3, {"ep": (z * ny + yy) * 2 + core})
     finish_first()
     send_back(0)
+    send_route_sums(0)
     finish_rest(1)
-    send_back(1)
     finish_rest(2)
     d = dfull[...].astype(BF16)
     dw_send[0 : 2 * ff, :] = dot_tn(d[:, 0 : 2 * ff], rows[:, 0:dq]).astype(BF16)
@@ -487,7 +507,11 @@
         mine = pl.ds(pl.multiple_of(t * ff + q * fo, 16), fo)
         own_grads.append(pltpu.make_async_copy(dw_send.at[mine, :], out.at[:, own_cols], in_sem.at[t]))
         own_grads[-1].start()
+    send_route_sums(1)
+    send_route_sums(2)
+    send_back(1)
     send_back(2)
+    spread_route_sums()
 
     if nz > 1:
         waits(sh3_recv.at[pl.ds(0, nz - 1)], SHARED_3, 1)
@@ -511,7 +535,7 @@
     own_grads[-1].start()
 
     waits(back_recv.at[pl.ds(0, (ep - 1) * cap)], BACK, 1)
-    waits(gp_recv.at[pl.ds(0, ep - 1)], GP, 1)
+    waits(gp_recv.at[:, pl.ds(0, nyc - 1)], GP + 2, 1)
     row_lane = lax.broadcasted_iota(I32, (1, 128), 1)
     comb[...] = jnp.zeros_like(comb)
     for t in range(tok):
@@ -520,7 +544,7 @@
             total = total + back_recv[slot_of[t, k]].astype(F32)
         comb[t] = total
         s = slot_of[t, q]
-        value = jnp.where(row_lane == s % cap, gp_recv[s // cap], 0.0)
+        value = jnp.where(row_lane == s % cap, gp_recv[s // (cap * nyc), (s // cap) % nyc], 0.0)
         grow[t : t + 1, :] = value
     gr_held[...] = jnp.sum(grow[...].T, axis=0, keepdims=True)[:, 0:tok] / weights[pl.ds(q, 1), :]
     swap_tok = swap_matrix(nb, 16)
@@ -557,7 +581,9 @@
     for n in range(2):
         waits(rest_recv.at[n, pl.ds(0, tp - 1)], SCATTER + 2 + 2 * n, 0)
     waits(back_send.at[pl.ds(0, (ep - 1) * cap)], BACK, 0)
-    waits(gp_send.at[pl.ds(0, ep - 1)], GP, 0)
+    if nz > 1:
+        waits(gp_mid.at[pl.ds(0, nz - 1)], GP, 0)
+    waits(gp_recv.at[:, pl.ds(0, nyc - 1)], GP + 2, 0)
     waits(sh4, SHARED_4, 0)
     waits(dw_send.at[pl.ds(0, 3 * (tp - 1) * fo), :], GRADS, 0)
     for copy in own_grads:
@@ -662,7 +688,8 @@
             pltpu.VMEM((slots, nb, 128), BF16),
             pltpu.VMEM((slots, nb, 128), BF16),
             pltpu.VMEM((ep, 1, 128), F32),
-            pltpu.VMEM((ep, 1, 128), F32),
+            pltpu.VMEM((nz, 2 * ny, 1, 128), F32),
+            pltpu.VMEM((nz, 2 * ny, 1, 128), F32),
             pltpu.VMEM((3 * ff, dq), BF16),
             pltpu.VMEM((tp, tok, dq), BF16),
             pltpu.VMEM((tp, tok, dq), BF16),

time: 61 us -> 58.2 us (0.954)
  Pallas kernels: 60.2 us -> 57.3 us
    pallas_call x1, Pallas kernels: 57.7 us -> 54.7 us  [local(): pl.pallas_call(functools.partial(kernel, sizes), out_shape=(jax.ShapeDtyp...]
where the time goes in v3:
time: 58.2 us; the launch traced here: 57.9 us
  Pallas kernels  57.3 us (98%)
  between operations  0.64 us (1%)
    pallas_call x1, Pallas kernels, local(): pl.pallas_call(functools.partial(kernel, sizes), out_shape=(jax.ShapeDtyp...  54.7 us
    pallas_call x1, Pallas kernels, local(): pl.pallas_call(functools.partial(finish, fo), out_shape=(jax.ShapeDtypeSt...  2.55 us

profile of v3, /device:TPU:1, one launch (start us, length us, event | category | flops | bytes accessed | tf_op | source)
XLA Modules:
  0.0 57.9 jit_solution(156395304178589987)
XLA Ops:
  0.6 54.7 %shard_map.161 = (bf16[24,1024]{1,0:T(8,128)(2,1)}, f32[1,24]{1,0:T(1,128)}, bf16[48,4096]{1,0:T(8,128)(2,1)}, bf16[48,4096]{1,0:T(8,128)(2,1)}, bf16[48,4096]{1,0:T(8,128)(2,1)}, /*index=5*/f32[144,64]{1,0:T(8,128)}) custom-call(s32[4,24]{1,0:T(4,128)} %bitcast.26, f32[4,24]{1,0:T(4,128)} %bitcast.27, bf16[24,4096]{1,0:T(8,128)(2,1)} %x_in.1, ...), custom_call_target="tpu_custom_call" | custom-call | tf_op jit(solution)/shard_map/pallas_call | solution.py:647
  55.4 2.6 %shard_map.162 = (bf16[24,1024]{1,0:T(8,128)(2,1)}, f32[1,24]{1,0:T(1,128)}, f32[48,4096]{1,0:T(8,128)}, f32[48,4096]{1,0:T(8,128)}, f32[48,4096]{1,0:T(8,128)},...) custom-call(bf16[24,1024]{1,0:T(8,128)(2,1)} %get-tuple-element.22.dx, f32[1,24]{1,0:T(1,128)} %get-tuple-element.23.gr, ...), custom_call_target="tpu_custom_call" | custom-call | tf_op jit(solution)/shard_map/pallas_call | solution.py:727

commit v4 on v3

--- a/solution.py
+++ b/solution.py
@@ -13,9 +13,12 @@
 I32 = jnp.int32
 EP_AXES = (8, 4, 2)
 CAP = 3
-(WEIGHTS, DISPATCH, SHARED_DX, SHARED_1, SHARED_2, SHARED_3, SHARED_4, SCATTER, GATHER, BACK, GP, GRADS) = range(
-    0, 72, 6
+(WEIGHTS, SHARED_DX, SHARED_1, SHARED_2, SHARED_3, SHARED_4, GATHER, BACK, GRADS, GP, DISPATCH, SCATTER) = (
+    *range(0, 20, 2),
+    22,
+    28,
 )
+PAIRS = 17
 
 
 def dot_nn(a, b):
@@ -48,12 +51,17 @@
 
 def z_order(nz):
     if nz == 8:
-        return (3, 5, 1, 7, 4, 0, 2, 6)
+        return (1, 7, 0, 2, 6, 3, 5, 4)
     return tuple(range(nz))
 
 
 def groups_of(ep):
-    return ((0, ep // 2), (ep // 2, ep // 4), (ep // 2 + ep // 4, ep // 4))
+    part = ep // 8
+    return ((0, 5 * part), (5 * part, 2 * part), (7 * part, part))
+
+
+def own_rows_of(first_rows, tp):
+    return -(-first_rows // (8 * tp)) * 8
 
 
 def kernel(
@@ -89,6 +97,7 @@
     sg_ref,
     su_ref,
     sd_ref,
+    staged,
     tiles,
     send_x,
     recv_x,
@@ -127,11 +136,12 @@
     in_sem,
 ):
     ep, tp, nz, ny, cap, tok, top, dq, ff, cb = sizes
+    slots = ep * cap
     nb = dq // 128
     nyc = 2 * ny
     groups = groups_of(ep)
     first_rows = groups[0][1] * cap
-    own_rows = first_rows // tp
+    own_rows = own_rows_of(first_rows, tp)
     fo = ff // tp
     chunk = cap * 2 * nb
     me = lax.axis_index("ep")
@@ -141,6 +151,8 @@
     yy = yc // 2
     zz = me // nyc
     sib = me + 1 - 2 * core
+
+    tp_order = sorted(range(1, tp), key=lambda i: -min(i, tp - i))
 
     def tp_peer(i):
         return lax.rem(q + i, tp)
@@ -198,10 +210,7 @@
                 (su_in, su_ref),
                 (sd_in, sd_ref),
             ]
-            + [
-                (ref.at[:, own_cols], wq.at[pl.ds(pl.multiple_of(t * ff + q * fo, 16), fo), :])
-                for t, ref in enumerate((wg_in, wu_in, wd_in))
-            ]
+            + [(ref, staged.at[t]) for t, ref in enumerate((wg_in, wu_in, wd_in))]
         )
     ]
     for fetch in fetches:
@@ -292,11 +301,13 @@
     pick(0)
     pl.semaphore_wait(barrier, ep - 1 + tp - 1)
 
-    for t, ref in enumerate((wg_in, wu_in, wd_in)):
-        for i in range(1, tp):
+    for n in (7, 8, 9):
+        fetches[n].wait()
+    for i in tp_order:
+        for t in range(3):
             dst_rows = pl.ds(pl.multiple_of(t * ff + q * fo, 16), fo)
             src_cols = pl.ds(pl.multiple_of(tp_peer(i) * dq, 128), dq)
-            send(ref.at[:, src_cols], wq.at[dst_rows, :], WEIGHTS, {"tp": tp_peer(i)})
+            send(staged.at[t, :, src_cols], wq.at[dst_rows, :], WEIGHTS, {"tp": tp_peer(i)})
     dispatch(0)
     pick(1)
     dispatch(1)
@@ -339,8 +350,15 @@
         y = lax.rem(yy + i, ny)
         send(sh2.at[y], sh2_recv.at[yy], SHARED_2, {"ep": (zz * ny + y) * 2 + core})
 
-    swap_in = swap_matrix(2 * nb, 16)
-    swap_back = swap_matrix(16, nb)
+    swap_in = {n: swap_matrix(2 * nb, n) for n in (8, 16)}
+    swap_back = {n: swap_matrix(n, nb) for n in (8, 16)}
+
+    def steps_of(base, count):
+        lo = base
+        while lo < base + count:
+            n = 16 if lo % 16 == 0 and lo + 16 <= base + count else 8
+            yield lo, n
+            lo += n
 
     def arrived(group):
         start, count = groups[group]
@@ -349,40 +367,52 @@
 
     def contract(group):
         base, count = groups[group][0] * cap, groups[group][1] * cap
-        for n in range(count // 16):
-            lo = base + n * 16
-            moved = dot_nn(swap_in, recv_x[lo * 2 * nb : (lo + 16) * 2 * nb, :]).astype(BF16)
+        for lo, n in steps_of(base, count):
+            moved = dot_nn(swap_in[n], recv_x[lo * 2 * nb : (lo + n) * 2 * nb, :])
             for b in range(2 * nb):
-                rows[lo : lo + 16, b * 128 : (b + 1) * 128] = moved[b * 16 : (b + 1) * 16]
+                rows[lo : lo + n, b * 128 : (b + 1) * 128] = moved[b * n : (b + 1) * n].astype(BF16)
         up_part = dot_nt(rows[base : base + count, 0:dq], wq[0 : 2 * ff, :])
         back_part = dot_nt(rows[base : base + count, dq : 2 * dq], wq[2 * ff : 3 * ff, :])
         return up_part, back_part
 
+    def packed_rows(n):
+        return n + -(-n // 16) * 8
+
+    def pack(ref, up, back):
+        n = up.shape[0]
+        half_n = packed_rows(n) - n
+        ref[0:n, :] = up.astype(ref.dtype)
+        ref[n : n + half_n, 0:ff] = back[0:half_n].astype(ref.dtype)
+        ref[n : n + n - half_n, ff : 2 * ff] = back[half_n:n].astype(ref.dtype)
+
+    def unpacked(total, n):
+        half_n = packed_rows(n) - n
+        back = jnp.concatenate([total[n : n + half_n, 0:ff], total[n : n + n - half_n, ff : 2 * ff]], axis=0)
+        return total[0:n, 0:ff], total[0:n, ff : 2 * ff], back
+
     def scatter_first():
         up_part, back_part = contract(0)
         for b in range(tp):
-            here = slice(b * own_rows, (b + 1) * own_rows)
-            part[b, :, 0 : 2 * ff] = up_part[here]
-            part[b, :, 2 * ff : 3 * ff] = back_part[here]
-            rs_send[b, :, 0 : 2 * ff] = up_part[here].astype(BF16)
-            rs_send[b, :, 2 * ff : 3 * ff] = back_part[here].astype(BF16)
-        for i in range(1, tp):
+            lo, hi = b * own_rows, min((b + 1) * own_rows, first_rows)
+            up, back = up_part[lo:hi], back_part[lo:hi]
+            if hi - lo < own_rows:
+                up = jnp.concatenate([up, jnp.zeros((own_rows - hi + lo, 2 * ff), F32)], axis=0)
+                back = jnp.concatenate([back, jnp.zeros((own_rows - hi + lo, ff), F32)], axis=0)
+            pack(part.at[b], up, back)
+            pack(rs_send.at[b], up, back)
+        for i in tp_order:
             send(rs_send.at[tp_peer(i)], rs_recv.at[q], SCATTER, {"tp": tp_peer(i)})
 
     def spread_rest(group):
         up_part, back_part = contract(group)
         n = group - 1
-        rest[n, :, 0 : 2 * ff] = up_part
-        rest[n, :, 2 * ff : 3 * ff] = back_part
-        rest_send[n, :, 0 : 2 * ff] = up_part.astype(BF16)
-        rest_send[n, :, 2 * ff : 3 * ff] = back_part.astype(BF16)
-        for i in range(1, tp):
-            send(rest_send.at[n], rest_recv.at[n, q], SCATTER + 2 * group, {"tp": tp_peer(i)})
-
-    def gradients(total):
-        gate = total[:, 0:ff]
-        up = total[:, ff : 2 * ff]
-        back = total[:, 2 * ff : 3 * ff]
+        pack(rest[n], up_part, back_part)
+        pack(rest_send[n], up_part, back_part)
+        for i in tp_order:
+            send(rest_send[n], rest_recv[n].at[q], SCATTER + 2 * group, {"tp": tp_peer(i)})
+
+    def gradients(total, n):
+        gate, up, back = unpacked(total, n)
         active, slope = swish_parts(gate)
         hidden = (active * up).astype(BF16).astype(F32)
         gp = jnp.sum(hidden * back, axis=1, keepdims=True)
@@ -396,36 +426,37 @@
         total = part[q]
         for i in range(1, tp):
             total = total + rs_recv[tp_peer(i)].astype(F32)
-        dall[q] = gradients(total).astype(BF16)
+        dall[q] = gradients(total, own_rows).astype(BF16)
         mine = dall.at[q]
-        for i in range(1, tp):
+        for i in tp_order:
             send(mine, mine, GATHER, {"tp": tp_peer(i)})
 
     def finish_first():
         waits(dall.at[pl.ds(0, tp - 1)], GATHER, 1)
         for b in range(tp):
-            dfull[b * own_rows : (b + 1) * own_rows, :] = dall[b].astype(F32)
+            lo, hi = b * own_rows, min((b + 1) * own_rows, first_rows)
+            dfull[lo:hi, :] = dall[b].astype(F32)[0 : hi - lo]
 
     def finish_rest(group):
         n = group - 1
-        waits(rest_recv.at[n, pl.ds(0, tp - 1)], SCATTER + 2 * group, 1)
-        total = rest[n]
+        waits(rest_recv[n].at[pl.ds(0, tp - 1)], SCATTER + 2 * group, 1)
+        total = rest[n][...]
         for i in range(1, tp):
-            total = total + rest_recv[n, tp_peer(i)].astype(F32)
+            total = total + rest_recv[n][tp_peer(i)].astype(F32)
         base, count = groups[group][0] * cap, groups[group][1] * cap
-        dfull[base : base + count, :] = gradients(total)
+        dfull[base : base + count, :] = gradients(total, count)
 
     def send_back(group):
         start, places = groups[group]
         base, count = start * cap, places * cap
         d = dfull[base : base + count, :]
         dxr = dot_nn(d[:, 0 : 2 * ff].astype(BF16), wq[0 : 2 * ff, :])
-        for n in range(count // 16):
+        for lo, n in steps_of(0, count):
             stacked = jnp.concatenate(
-                [dxr[n * 16 : (n + 1) * 16, b * 128 : (b + 1) * 128] for b in range(nb)], axis=0
+                [dxr[lo : lo + n, b * 128 : (b + 1) * 128] for b in range(nb)], axis=0
             ).astype(BF16)
-            moved = dot_nn(swap_back, stacked)
-            back_send[base + n * 16 : base + (n + 1) * 16] = moved.reshape(16, nb, 128).astype(BF16)
+            moved = dot_nn(swap_back[n], stacked)
+            back_send[base + lo : base + lo + n] = moved.reshape(n, nb, 128).astype(BF16)
         for lo, hi, dz, place in positions(group):
             if dz == 0 and lo == 0:
                 back_recv[pl.ds(me * cap, cap)] = back_send[place * cap : (place + 1) * cap]
@@ -470,16 +501,16 @@
         gp_recv[:, yc] = gp_mid[:, 0]
 
     arrived(0)
-    for n in (7, 8, 9):
-        fetches[n].wait()
+    for t in range(3):
+        wq[pl.ds(pl.multiple_of(t * ff + q * fo, 16), fo), :] = staged[t, :, own_cols]
     waits(wq.at[pl.ds(0, 3 * (tp - 1) * fo), :], WEIGHTS, 1)
     scatter_first()
-    gather_first()
     arrived(1)
     spread_rest(1)
+    gather_first()
     arrived(2)
     spread_rest(2)
-    for i in range(1, tp):
+    for i in tp_order:
         send(sdx_send.at[tp_peer(i)], sdx_recv.at[q], SHARED_DX, {"tp": tp_peer(i)})
     if ny > 1:
         waits(sh2_recv.at[pl.ds(0, ny - 1)], SHARED_2, 1)
@@ -491,26 +522,31 @@
     for i in range(1, nz):
         z = lax.rem(zz + i, nz)
         send(sh3.at[z], sh3_recv.at[zz], SHARED_3, {"ep": (z * ny + yy) * 2 + core})
+    finish_rest(1)
+    send_route_sums(1)
+    send_back(1)
     finish_first()
-    send_back(0)
-    send_route_sums(0)
-    finish_rest(1)
     finish_rest(2)
-    d = dfull[...].astype(BF16)
-    dw_send[0 : 2 * ff, :] = dot_tn(d[:, 0 : 2 * ff], rows[:, 0:dq]).astype(BF16)
-    dw_send[2 * ff : 3 * ff, :] = dot_tn(d[:, 2 * ff : 3 * ff], rows[:, dq : 2 * dq]).astype(BF16)
+    d = dfull[:, 0 : 3 * ff].astype(BF16)
     own_grads = []
-    for t, out in enumerate((gg_out, gu_out, gd_out)):
-        for i in range(1, tp):
+
+    def send_grads(t, out):
+        for i in tp_order:
             src_rows = pl.ds(pl.multiple_of(t * ff + tp_peer(i) * fo, 16), fo)
             send(dw_send.at[src_rows, :], out.at[:, own_cols], GRADS, {"tp": tp_peer(i)})
         mine = pl.ds(pl.multiple_of(t * ff + q * fo, 16), fo)
         own_grads.append(pltpu.make_async_copy(dw_send.at[mine, :], out.at[:, own_cols], in_sem.at[t]))
         own_grads[-1].start()
-    send_route_sums(1)
+
+    dw_send[2 * ff : 3 * ff, :] = dot_tn(d[:, 2 * ff : 3 * ff], rows[:, dq : 2 * dq]).astype(BF16)
+    send_grads(2, gd_out)
+    dw_send[0 : 2 * ff, :] = dot_tn(d[:, 0 : 2 * ff], rows[:, 0:dq]).astype(BF16)
+    send_grads(0, gg_out)
+    send_grads(1, gu_out)
     send_route_sums(2)
-    send_back(1)
+    send_route_sums(0)
     send_back(2)
+    send_back(0)
     spread_route_sums()
 
     if nz > 1:
@@ -579,7 +615,7 @@
     waits(rs_send.at[pl.ds(0, tp - 1)], SCATTER, 0)
     waits(dall.at[pl.ds(0, tp - 1)], GATHER, 0)
     for n in range(2):
-        waits(rest_recv.at[n, pl.ds(0, tp - 1)], SCATTER + 2 + 2 * n, 0)
+        waits(rest_recv[n].at[pl.ds(0, tp - 1)], SCATTER + 2 + 2 * n, 0)
     waits(back_send.at[pl.ds(0, (ep - 1) * cap)], BACK, 0)
     if nz > 1:
         waits(gp_mid.at[pl.ds(0, nz - 1)], GP, 0)
@@ -591,27 +627,20 @@
     waits(dw_send.at[pl.ds(0, 3 * (tp - 1) * fo), :], GRADS, 1)
 
 
-def finish(fo, dx, gr, gg, gu, gd, gs, dx_o, gr_o, gg_o, gu_o, gd_o, gsg_o, gsu_o, gsd_o, narrow, wide, small, sem):
+def finish(fo, dx, gr, gg, gu, gd, gs, dx_o, gr_o, gg_o, gu_o, gd_o, gsg_o, gsu_o, gsd_o, wide, small, sem):
     width = gg.shape[1]
     parts = 2
     step = width // parts
-    loads = []
-    for t, src in enumerate((gg, gu, gd)):
-        for c in range(parts):
-            cols = slice(c * step, (c + 1) * step)
-            loads.append(pltpu.make_async_copy(src.at[:, cols], narrow.at[t, :, cols], sem.at[t * parts + c]))
-            loads[-1].start()
     last = 6 * parts
     others = [(gs, small[0]), (dx, small[1]), (gr, small[2])]
     ins = [pltpu.make_async_copy(src, dst, sem.at[last + n]) for n, (src, dst) in enumerate(others)]
     for copy in ins:
         copy.start()
     stores = []
-    for t, dst in enumerate((gg_o, gu_o, gd_o)):
+    for t, (src, dst) in enumerate(((gg, gg_o), (gu, gu_o), (gd, gd_o))):
         for c in range(parts):
             cols = slice(c * step, (c + 1) * step)
-            loads[t * parts + c].wait()
-            wide[t, :, cols] = narrow[t, :, cols].astype(F32)
+            wide[t, :, cols] = src[:, cols].astype(F32)
             stores.append(pltpu.make_async_copy(wide.at[t, :, cols], dst.at[:, cols], sem.at[(3 + t) * parts + c]))
             stores[-1].start()
     for copy in ins:
@@ -637,7 +666,10 @@
     nb = dq // 128
     cb = width // (nz * ny)
     slots = ep * cap
-    own_rows = slots // tp // 2
+    groups = groups_of(ep)
+    own_rows = own_rows_of(groups[0][1] * cap, tp)
+    taller = lambda n: n + -(-n // 16) * 8
+    rest_rows = [count * cap for _, count in groups[1:]]
     wide = -(-(3 * ff + 1) // 128) * 128
     half = 3 * fo // 2
 
@@ -655,7 +687,7 @@
             jax.ShapeDtypeStruct((3 * fo, cb // 2), F32),
         ),
         in_specs=[hbm] * 10,
-        out_specs=(hbm,) * 6,
+        out_specs=(hbm, hbm, vmem, vmem, vmem, hbm),
         scratch_shapes=[
             pltpu.VMEM((top, tok), I32),
             pltpu.VMEM((top, tok), F32),
@@ -672,17 +704,18 @@
             pltpu.VMEM((fo, width), BF16),
             pltpu.VMEM((fo, width), BF16),
             pltpu.VMEM((fo, width), BF16),
+            pltpu.VMEM((3, fo, width), BF16),
             pltpu.VMEM((32, 2 * nb, 128), F32),
             pltpu.VMEM((slots * 2 * nb, 128), BF16),
             pltpu.VMEM((slots * 2 * nb, 128), BF16),
             pltpu.VMEM((3 * ff, dq), BF16),
             pltpu.VMEM((slots, 2 * dq), BF16),
-            pltpu.VMEM((tp, own_rows, 3 * ff), F32),
-            pltpu.VMEM((tp, own_rows, 3 * ff), BF16),
-            pltpu.VMEM((tp, own_rows, 3 * ff), BF16),
-            pltpu.VMEM((2, slots // 4, 3 * ff), F32),
-            pltpu.VMEM((2, slots // 4, 3 * ff), BF16),
-            pltpu.VMEM((2, tp, slots // 4, 3 * ff), BF16),
+            pltpu.VMEM((tp, taller(own_rows), 2 * ff), F32),
+            pltpu.VMEM((tp, taller(own_rows), 2 * ff), BF16),
+            pltpu.VMEM((tp, taller(own_rows), 2 * ff), BF16),
+            [pltpu.VMEM((taller(n), 2 * ff), F32) for n in rest_rows],
+            [pltpu.VMEM((taller(n), 2 * ff), BF16) for n in rest_rows],
+            [pltpu.VMEM((tp, taller(n), 2 * ff), BF16) for n in rest_rows],
             pltpu.VMEM((tp, own_rows, wide), BF16),
             pltpu.VMEM((slots, wide), F32),
             pltpu.VMEM((slots, nb, 128), BF16),
@@ -706,13 +739,14 @@
             pltpu.VMEM((3 * fo, cb // 2), F32),
             pltpu.VMEM((tok, dq), BF16),
             pltpu.VMEM((1, tok), F32),
-            pltpu.SemaphoreType.DMA((72,)),
+            pltpu.SemaphoreType.DMA((2 * PAIRS,)),
             pltpu.SemaphoreType.DMA((13,)),
         ],
         compiler_params=pltpu.CompilerParams(
-            collective_id=0, has_side_effects=True, vmem_limit_bytes=67043328
+            collective_id=0, has_side_effects=True, vmem_limit_bytes=50*1024*1024
         ),
     )(
+        *[pltpu.with_memory_space_constraint(a, pltpu.HBM) for a in (
         routes.T,
         route_weights.T,
         tokens,
@@ -723,6 +757,7 @@
         shared_gate.T,
         shared_up.T,
         shared_down,
+        )]
     )
     dx, gr, gg, gu, gd, gsg, gsu, gsd = pl.pallas_call(
         functools.partial(finish, fo),
@@ -736,15 +771,14 @@
             jax.ShapeDtypeStruct((fo, cb // 2), F32),
             jax.ShapeDtypeStruct((fo, cb // 2), F32),
         ),
-        in_specs=[hbm] * 6,
+        in_specs=[hbm, hbm, vmem, vmem, vmem, hbm],
         out_specs=(hbm,) * 8,
         scratch_shapes=[
-            pltpu.VMEM((3, fo, width), BF16),
             pltpu.VMEM((3, fo, width), F32),
             [pltpu.VMEM((3 * fo, cb // 2), F32), pltpu.VMEM((tok, dq), BF16), pltpu.VMEM((1, tok), F32)],
             pltpu.SemaphoreType.DMA((20,)),
         ],
-        compiler_params=pltpu.CompilerParams(vmem_limit_bytes=67043328),
+        compiler_params=pltpu.CompilerParams(vmem_limit_bytes=16*1024*1024),
     )(*outs)
     return (dx, gr.T, gg.T[None], gu.T[None], gd[None], gsg.T, gsu.T, gsd)
 

time: 58.2 us -> 56 us (0.962)
  Pallas kernels: 57.3 us -> 55.3 us
    pallas_call x1, Pallas kernels: 54.7 us -> 53.5 us  [local(): pl.pallas_call(functools.partial(kernel, sizes), out_shape=(jax.ShapeDtyp...]
    pallas_call x1, Pallas kernels: 2.55 us -> 1.78 us  [local(): pl.pallas_call(functools.partial(finish, fo), out_shape=(jax.ShapeDtypeSt...]
where the time goes in v4:
time: 56 us; the launch traced here: 55.9 us
  Pallas kernels  55.3 us (99%)
  between operations  0.64 us (1%)
    pallas_call x1, Pallas kernels, local(): pl.pallas_call(functools.partial(kernel, sizes), out_shape=(jax.ShapeDtyp...  53.5 us
    pallas_call x1, Pallas kernels, local(): pl.pallas_call(functools.partial(finish, fo), out_shape=(jax.ShapeDtypeSt...  1.78 us

profile of v4, /device:TPU:1, one launch (start us, length us, event | category | flops | bytes accessed | tf_op | source)
XLA Modules:
  0.0 55.9 jit_solution(7314432885459839896)
XLA Ops:
  0.6 53.5 %shard_map.161 = (bf16[24,1024]{1,0:T(8,128)(2,1)S(1)}, f32[1,24]{1,0:T(1,128)S(1)}, bf16[48,4096]{1,0:T(8,128)(2,1)S(1)}, bf16[48,4096]{1,0:T(8,128)(2,1)S(1)},...) custom-call(s32[4,24]{1,0:T(4,128)} %bitcast.26, f32[4,24]{1,0:T(4,128)} %bitcast.27, bf16[24,4096]{1,0:T(8,128)(2,1)} %x_in.1, ...), custom_call_target="tpu_custom_call" | custom-call | tf_op jit(solution)/shard_map/pallas_call | solution.py:679
  54.1 1.8 %shard_map.162 = (bf16[24,1024]{1,0:T(8,128)(2,1)}, f32[1,24]{1,0:T(1,128)}, f32[48,4096]{1,0:T(8,128)}, f32[48,4096]{1,0:T(8,128)}, f32[48,4096]{1,0:T(8,128)},...) custom-call(bf16[24,1024]{1,0:T(8,128)(2,1)S(1)} %get-tuple-element.22.dx, ...), custom_call_target="tpu_custom_call" | custom-call | tf_op jit(solution)/shard_map/pallas_call | solution.py:762

commit v5 on v4

--- a/solution.py
+++ b/solution.py
@@ -18,7 +18,8 @@
     22,
     28,
 )
-PAIRS = 17
+DOWN, SCATTER_BACK = 34, 36
+PAIRS = 19
 
 
 def dot_nn(a, b):
@@ -303,11 +304,12 @@
 
     for n in (7, 8, 9):
         fetches[n].wait()
-    for i in tp_order:
-        for t in range(3):
-            dst_rows = pl.ds(pl.multiple_of(t * ff + q * fo, 16), fo)
-            src_cols = pl.ds(pl.multiple_of(tp_peer(i) * dq, 128), dq)
-            send(staged.at[t, :, src_cols], wq.at[dst_rows, :], WEIGHTS, {"tp": tp_peer(i)})
+    for types, kind in (((0, 1), WEIGHTS), ((2,), DOWN)):
+        for i in tp_order:
+            for t in types:
+                dst_rows = pl.ds(pl.multiple_of(t * ff + q * fo, 16), fo)
+                src_cols = pl.ds(pl.multiple_of(tp_peer(i) * dq, 128), dq)
+                send(staged.at[t, :, src_cols], wq.at[dst_rows, :], kind, {"tp": tp_peer(i)})
     dispatch(0)
     pick(1)
     dispatch(1)
@@ -365,12 +367,16 @@
         own = 1 if start <= own_place < start + count else 0
         waits(recv_x.at[pl.ds(0, (count - own) * chunk), :], DISPATCH + 2 * group, 1)
 
-    def contract(group):
+    def relayout(group):
         base, count = groups[group][0] * cap, groups[group][1] * cap
         for lo, n in steps_of(base, count):
             moved = dot_nn(swap_in[n], recv_x[lo * 2 * nb : (lo + n) * 2 * nb, :])
             for b in range(2 * nb):
                 rows[lo : lo + n, b * 128 : (b + 1) * 128] = moved[b * n : (b + 1) * n].astype(BF16)
+
+    def contract(group):
+        base, count = groups[group][0] * cap, groups[group][1] * cap
+        relayout(group)
         up_part = dot_nt(rows[base : base + count, 0:dq], wq[0 : 2 * ff, :])
         back_part = dot_nt(rows[base : base + count, dq : 2 * dq], wq[2 * ff : 3 * ff, :])
         return up_part, back_part
@@ -390,18 +396,34 @@
         back = jnp.concatenate([total[n : n + half_n, 0:ff], total[n : n + n - half_n, ff : 2 * ff]], axis=0)
         return total[0:n, 0:ff], total[0:n, ff : 2 * ff], back
 
-    def scatter_first():
-        up_part, back_part = contract(0)
+    own_tall = packed_rows(own_rows)
+
+    def blocks_of(whole):
         for b in range(tp):
             lo, hi = b * own_rows, min((b + 1) * own_rows, first_rows)
-            up, back = up_part[lo:hi], back_part[lo:hi]
+            block = whole[lo:hi]
             if hi - lo < own_rows:
-                up = jnp.concatenate([up, jnp.zeros((own_rows - hi + lo, 2 * ff), F32)], axis=0)
-                back = jnp.concatenate([back, jnp.zeros((own_rows - hi + lo, ff), F32)], axis=0)
-            pack(part.at[b], up, back)
-            pack(rs_send.at[b], up, back)
+                block = jnp.concatenate([block, jnp.zeros((own_rows - hi + lo, whole.shape[1]), F32)], axis=0)
+            yield b, block
+
+    def scatter_up():
+        relayout(0)
+        for b, block in blocks_of(dot_nt(rows[0:first_rows, 0:dq], wq[0 : 2 * ff, :])):
+            part[b, 0:own_rows, :] = block
+            rs_send[b, 0:own_rows, :] = block.astype(BF16)
+        here = pl.ds(0, own_rows)
         for i in tp_order:
-            send(rs_send.at[tp_peer(i)], rs_recv.at[q], SCATTER, {"tp": tp_peer(i)})
+            send(rs_send.at[tp_peer(i), here], rs_recv.at[q, here], SCATTER, {"tp": tp_peer(i)})
+
+    def scatter_back():
+        half_n = own_tall - own_rows
+        for b, block in blocks_of(dot_nt(rows[0:first_rows, dq : 2 * dq], wq[2 * ff : 3 * ff, :])):
+            for ref in (part, rs_send):
+                ref[b, own_rows:own_tall, 0:ff] = block[0:half_n].astype(ref.dtype)
+                ref[b, own_rows : 2 * own_rows - half_n, ff : 2 * ff] = block[half_n:own_rows].astype(ref.dtype)
+        here = pl.ds(own_rows, half_n)
+        for i in tp_order:
+            send(rs_send.at[tp_peer(i), here], rs_recv.at[q, here], SCATTER_BACK, {"tp": tp_peer(i)})
 
     def spread_rest(group):
         up_part, back_part = contract(group)
@@ -422,7 +444,8 @@
         )
 
     def gather_first():
-        waits(rs_recv.at[pl.ds(0, tp - 1)], SCATTER, 1)
+        waits(rs_recv.at[pl.ds(0, tp - 1), pl.ds(0, own_rows)], SCATTER, 1)
+        waits(rs_recv.at[pl.ds(0, tp - 1), pl.ds(own_rows, own_tall - own_rows)], SCATTER_BACK, 1)
         total = part[q]
         for i in range(1, tp):
             total = total + rs_recv[tp_peer(i)].astype(F32)
@@ -500,14 +523,16 @@
             send(gp_mid.at[:, w], gp_recv.at[:, yc], GP + 2, {"ep": from_of(0, w)})
         gp_recv[:, yc] = gp_mid[:, 0]
 
-    arrived(0)
     for t in range(3):
         wq[pl.ds(pl.multiple_of(t * ff + q * fo, 16), fo), :] = staged[t, :, own_cols]
-    waits(wq.at[pl.ds(0, 3 * (tp - 1) * fo), :], WEIGHTS, 1)
-    scatter_first()
+    waits(wq.at[pl.ds(0, 2 * (tp - 1) * fo), :], WEIGHTS, 1)
+    arrived(0)
+    scatter_up()
+    waits(wq.at[pl.ds(0, (tp - 1) * fo), :], DOWN, 1)
+    scatter_back()
+    gather_first()
     arrived(1)
     spread_rest(1)
-    gather_first()
     arrived(2)
     spread_rest(2)
     for i in tp_order:
@@ -602,7 +627,8 @@
     for n, (src, dst) in enumerate(((dx_held, dx_out), (gr_held, gr_out))):
         own_grads.append(pltpu.make_async_copy(src, dst, in_sem.at[4 + n]))
         own_grads[-1].start()
-    waits(wq.at[pl.ds(0, 3 * (tp - 1) * fo), :], WEIGHTS, 0)
+    waits(wq.at[pl.ds(0, 2 * (tp - 1) * fo), :], WEIGHTS, 0)
+    waits(wq.at[pl.ds(0, (tp - 1) * fo), :], DOWN, 0)
     for group, (start, count) in enumerate(groups):
         own = 1 if start <= own_place < start + count else 0
         waits(send_x.at[pl.ds(0, (count - own) * chunk), :], DISPATCH + 2 * group, 0)
@@ -612,7 +638,8 @@
         waits(sh2.at[pl.ds(0, ny - 1)], SHARED_2, 0)
     if nz > 1:
         waits(sh3.at[pl.ds(0, nz - 1)], SHARED_3, 0)
-    waits(rs_send.at[pl.ds(0, tp - 1)], SCATTER, 0)
+    waits(rs_send.at[pl.ds(0, tp - 1), pl.ds(0, own_rows)], SCATTER, 0)
+    waits(rs_send.at[pl.ds(0, tp - 1), pl.ds(own_rows, own_tall - own_rows)], SCATTER_BACK, 0)
     waits(dall.at[pl.ds(0, tp - 1)], GATHER, 0)
     for n in range(2):
         waits(rest_recv[n].at[pl.ds(0, tp - 1)], SCATTER + 2 + 2 * n, 0)

time: 56 us -> 54.6 us (0.975)
  Pallas kernels: 55.3 us -> 53.6 us
    pallas_call x1, Pallas kernels: 53.5 us -> 51.8 us  [local(): pl.pallas_call(functools.partial(kernel, sizes), out_shape=(jax.ShapeDtyp...]
where the time goes in v5:
time: 54.6 us; the launch traced here: 54.2 us
  Pallas kernels  53.6 us (98%)
  between operations  0.64 us (1%)
    pallas_call x1, Pallas kernels, local(): pl.pallas_call(functools.partial(kernel, sizes), out_shape=(jax.ShapeDtyp...  51.8 us
    pallas_call x1, Pallas kernels, local(): pl.pallas_call(functools.partial(finish, fo), out_shape=(jax.ShapeDtypeSt...  1.78 us

profile of v5, /device:TPU:1, one launch (start us, length us, event | category | flops | bytes accessed | tf_op | source)
XLA Modules:
  0.0 54.2 jit_solution(5689274327018270894)
XLA Ops:
  0.6 51.8 %shard_map.161 = (bf16[24,1024]{1,0:T(8,128)(2,1)S(1)}, f32[1,24]{1,0:T(1,128)S(1)}, bf16[48,4096]{1,0:T(8,128)(2,1)S(1)}, bf16[48,4096]{1,0:T(8,128)(2,1)S(1)},...) custom-call(s32[4,24]{1,0:T(4,128)} %bitcast.26, f32[4,24]{1,0:T(4,128)} %bitcast.27, bf16[24,4096]{1,0:T(8,128)(2,1)} %x_in.1, ...), custom_call_target="tpu_custom_call" | custom-call | tf_op jit(solution)/shard_map/pallas_call | solution.py:706
  52.4 1.8 %shard_map.162 = (bf16[24,1024]{1,0:T(8,128)(2,1)}, f32[1,24]{1,0:T(1,128)}, f32[48,4096]{1,0:T(8,128)}, f32[48,4096]{1,0:T(8,128)}, f32[48,4096]{1,0:T(8,128)},...) custom-call(bf16[24,1024]{1,0:T(8,128)(2,1)S(1)} %get-tuple-element.22.dx, ...), custom_call_target="tpu_custom_call" | custom-call | tf_op jit(solution)/shard_map/pallas_call | solution.py:789

commit v6 on v5

--- a/solution.py
+++ b/solution.py
@@ -302,6 +302,7 @@
     pick(0)
     pl.semaphore_wait(barrier, ep - 1 + tp - 1)
 
+    dispatch(0)
     for n in (7, 8, 9):
         fetches[n].wait()
     for types, kind in (((0, 1), WEIGHTS), ((2,), DOWN)):
@@ -310,7 +311,6 @@
                 dst_rows = pl.ds(pl.multiple_of(t * ff + q * fo, 16), fo)
                 src_cols = pl.ds(pl.multiple_of(tp_peer(i) * dq, 128), dq)
                 send(staged.at[t, :, src_cols], wq.at[dst_rows, :], kind, {"tp": tp_peer(i)})
-    dispatch(0)
     pick(1)
     dispatch(1)
     pick(2)
@@ -658,9 +658,8 @@
     width = gg.shape[1]
     parts = 2
     step = width // parts
-    last = 6 * parts
     others = [(gs, small[0]), (dx, small[1]), (gr, small[2])]
-    ins = [pltpu.make_async_copy(src, dst, sem.at[last + n]) for n, (src, dst) in enumerate(others)]
+    ins = [pltpu.make_async_copy(src, dst, sem.at[1 + n]) for n, (src, dst) in enumerate(others)]
     for copy in ins:
         copy.start()
     stores = []
@@ -668,17 +667,17 @@
         for c in range(parts):
             cols = slice(c * step, (c + 1) * step)
             wide[t, :, cols] = src[:, cols].astype(F32)
-            stores.append(pltpu.make_async_copy(wide.at[t, :, cols], dst.at[:, cols], sem.at[(3 + t) * parts + c]))
-            stores[-1].start()
+            pltpu.make_async_copy(wide.at[t, :, cols], dst.at[:, cols], sem.at[0]).start()
     for copy in ins:
         copy.wait()
     outs = [(small[0].at[t * fo : (t + 1) * fo], dst) for t, dst in enumerate((gsg_o, gsu_o, gsd_o))]
     outs += [(small[1], dx_o), (small[2], gr_o)]
     for n, (src, dst) in enumerate(outs):
-        stores.append(pltpu.make_async_copy(src, dst, sem.at[last + 3 + n]))
+        stores.append(pltpu.make_async_copy(src, dst, sem.at[4 + n]))
         stores[-1].start()
     for copy in stores:
         copy.wait()
+    wait_bytes(wide, sem.at[0])
 
 
 def local(axes, cap, tokens, cotangent, routes, route_weights, expert_gate, expert_up, expert_down, shared_gate, shared_up, shared_down):
@@ -803,7 +802,7 @@
         scratch_shapes=[
             pltpu.VMEM((3, fo, width), F32),
             [pltpu.VMEM((3 * fo, cb // 2), F32), pltpu.VMEM((tok, dq), BF16), pltpu.VMEM((1, tok), F32)],
-            pltpu.SemaphoreType.DMA((20,)),
+            pltpu.SemaphoreType.DMA((9,)),
         ],
         compiler_params=pltpu.CompilerParams(vmem_limit_bytes=16*1024*1024),
     )(*outs)

time: 54.6 us -> 54.6 us (level)
  no operation moved by 1% of the time
where the time goes in v6:
time: 54.6 us; the launch traced here: 54.5 us
  Pallas kernels  53.8 us (99%)
  between operations  0.64 us (1%)
    pallas_call x1, Pallas kernels, local(): pl.pallas_call(functools.partial(kernel, sizes), out_shape=(jax.ShapeDtyp...  52.1 us
    pallas_call x1, Pallas kernels, local(): pl.pallas_call(functools.partial(finish, fo), out_shape=(jax.ShapeDtypeSt...  1.69 us

profile of v6, /device:TPU:1, one launch (start us, length us, event | category | flops | bytes accessed | tf_op | source)
XLA Modules:
  0.0 54.5 jit_solution(11660569193401469037)
XLA Ops:
  0.6 52.1 %shard_map.161 = (bf16[24,1024]{1,0:T(8,128)(2,1)S(1)}, f32[1,24]{1,0:T(1,128)S(1)}, bf16[48,4096]{1,0:T(8,128)(2,1)S(1)}, bf16[48,4096]{1,0:T(8,128)(2,1)S(1)},...) custom-call(s32[4,24]{1,0:T(4,128)} %bitcast.26, f32[4,24]{1,0:T(4,128)} %bitcast.27, bf16[24,4096]{1,0:T(8,128)(2,1)} %x_in.1, ...), custom_call_target="tpu_custom_call" | custom-call | tf_op jit(solution)/shard_map/pallas_call | solution.py:705
  52.8 1.7 %shard_map.162 = (bf16[24,1024]{1,0:T(8,128)(2,1)}, f32[1,24]{1,0:T(1,128)}, f32[48,4096]{1,0:T(8,128)}, f32[48,4096]{1,0:T(8,128)}, f32[48,4096]{1,0:T(8,128)},...) custom-call(bf16[24,1024]{1,0:T(8,128)(2,1)S(1)} %get-tuple-element.22.dx, ...), custom_call_target="tpu_custom_call" | custom-call | tf_op jit(solution)/shard_map/pallas_call | solution.py:788

commit v7 on v6

--- a/solution.py
+++ b/solution.py
@@ -530,13 +530,13 @@
     scatter_up()
     waits(wq.at[pl.ds(0, (tp - 1) * fo), :], DOWN, 1)
     scatter_back()
+    for i in tp_order:
+        send(sdx_send.at[tp_peer(i)], sdx_recv.at[q], SHARED_DX, {"tp": tp_peer(i)})
     gather_first()
     arrived(1)
     spread_rest(1)
     arrived(2)
     spread_rest(2)
-    for i in tp_order:
-        send(sdx_send.at[tp_peer(i)], sdx_recv.at[q], SHARED_DX, {"tp": tp_peer(i)})
     if ny > 1:
         waits(sh2_recv.at[pl.ds(0, ny - 1)], SHARED_2, 1)
     for z in range(nz):

time: 54.6 us -> 54.5 us (level)
  no operation moved by 1% of the time
where the time goes in v7:
time: 54.5 us; the launch traced here: 54.4 us
  Pallas kernels  53.7 us (99%)
  between operations  0.64 us (1%)
    pallas_call x1, Pallas kernels, local(): pl.pallas_call(functools.partial(kernel, sizes), out_shape=(jax.ShapeDtyp...  52 us
    pallas_call x1, Pallas kernels, local(): pl.pallas_call(functools.partial(finish, fo), out_shape=(jax.ShapeDtypeSt...  1.69 us

profile of v7, /device:TPU:1, one launch (start us, length us, event | category | flops | bytes accessed | tf_op | source)
XLA Modules:
  0.0 54.4 jit_solution(5712547259706651344)
XLA Ops:
  0.6 52.0 %shard_map.161 = (bf16[24,1024]{1,0:T(8,128)(2,1)S(1)}, f32[1,24]{1,0:T(1,128)S(1)}, bf16[48,4096]{1,0:T(8,128)(2,1)S(1)}, bf16[48,4096]{1,0:T(8,128)(2,1)S(1)},...) custom-call(s32[4,24]{1,0:T(4,128)} %bitcast.26, f32[4,24]{1,0:T(4,128)} %bitcast.27, bf16[24,4096]{1,0:T(8,128)(2,1)} %x_in.1, ...), custom_call_target="tpu_custom_call" | custom-call | tf_op jit(solution)/shard_map/pallas_call | solution.py:705
  52.7 1.7 %shard_map.162 = (bf16[24,1024]{1,0:T(8,128)(2,1)}, f32[1,24]{1,0:T(1,128)}, f32[48,4096]{1,0:T(8,128)}, f32[48,4096]{1,0:T(8,128)}, f32[48,4096]{1,0:T(8,128)},...) custom-call(bf16[24,1024]{1,0:T(8,128)(2,1)S(1)} %get-tuple-element.22.dx, ...), custom_call_target="tpu_custom_call" | custom-call | tf_op jit(solution)/shard_map/pallas_call | solution.py:788

commit v8 on v7

--- a/solution.py
+++ b/solution.py
@@ -547,10 +547,10 @@
     for i in range(1, nz):
         z = lax.rem(zz + i, nz)
         send(sh3.at[z], sh3_recv.at[zz], SHARED_3, {"ep": (z * ny + yy) * 2 + core})
+    finish_first()
+    send_route_sums(0)
+    send_back(0)
     finish_rest(1)
-    send_route_sums(1)
-    send_back(1)
-    finish_first()
     finish_rest(2)
     d = dfull[:, 0 : 3 * ff].astype(BF16)
     own_grads = []
@@ -569,9 +569,9 @@
     send_grads(0, gg_out)
     send_grads(1, gu_out)
     send_route_sums(2)
-    send_route_sums(0)
+    send_route_sums(1)
     send_back(2)
-    send_back(0)
+    send_back(1)
     spread_route_sums()
 
     if nz > 1:

time: 54.5 us -> 55.1 us (1.011)
  Pallas kernels: 53.7 us -> 54.4 us
    pallas_call x1, Pallas kernels: 52 us -> 52.7 us  [local(): pl.pallas_call(functools.partial(kernel, sizes), out_shape=(jax.ShapeDtyp...]
where the time goes in v8:
time: 55.1 us; the launch traced here: 55 us
  Pallas kernels  54.4 us (99%)
  between operations  0.64 us (1%)
    pallas_call x1, Pallas kernels, local(): pl.pallas_call(functools.partial(kernel, sizes), out_shape=(jax.ShapeDtyp...  52.7 us
    pallas_call x1, Pallas kernels, local(): pl.pallas_call(functools.partial(finish, fo), out_shape=(jax.ShapeDtypeSt...  1.69 us

profile of v8, /device:TPU:1, one launch (start us, length us, event | category | flops | bytes accessed | tf_op | source)
XLA Modules:
  0.0 55.0 jit_solution(4994505926768770559)
XLA Ops:
  0.6 52.7 %shard_map.161 = (bf16[24,1024]{1,0:T(8,128)(2,1)S(1)}, f32[1,24]{1,0:T(1,128)S(1)}, bf16[48,4096]{1,0:T(8,128)(2,1)S(1)}, bf16[48,4096]{1,0:T(8,128)(2,1)S(1)},...) custom-call(s32[4,24]{1,0:T(4,128)} %bitcast.26, f32[4,24]{1,0:T(4,128)} %bitcast.27, bf16[24,4096]{1,0:T(8,128)(2,1)} %x_in.1, ...), custom_call_target="tpu_custom_call" | custom-call | tf_op jit(solution)/shard_map/pallas_call | solution.py:705
  53.3 1.7 %shard_map.162 = (bf16[24,1024]{1,0:T(8,128)(2,1)}, f32[1,24]{1,0:T(1,128)}, f32[48,4096]{1,0:T(8,128)}, f32[48,4096]{1,0:T(8,128)}, f32[48,4096]{1,0:T(8,128)},...) custom-call(bf16[24,1024]{1,0:T(8,128)(2,1)S(1)} %get-tuple-element.22.dx, ...), custom_call_target="tpu_custom_call" | custom-call | tf_op jit(solution)/shard_map/pallas_call | solution.py:788
